TPU v7x, 32 devices: a whole 2x2x4 slice. The times are simulated.
32 devices in a mesh: ep: 8 (over z, y), tp: 4 (over x, core).
Axes of the slice: x: 2, y: 2, z: 4, core: 2. Of those that a mesh axis runs over, the one named last changes fastest.
Arguments:
- mixer_in: bfloat16 [4096, 4096], P(('ep', 'tp')), may hold values from -6 to 6
- mixer_gain: float32 [4096], replicated, may hold values from 0.1 to 1.9
- group_weight: bfloat16 [4, 1024, 1024], P('tp'), may hold values from -0.1875 to 0.1875
- group_scale: float32 [4, 1024], P('tp'), may hold values from 0.1 to 1.9
- expert_in: bfloat16 [4096, 4096], P(('ep', 'tp')), may hold values from -6 to 6
- expert_gain: float32 [4096], replicated, may hold values from 0.1 to 1.9
- routes: int32 [4096, 2], P('ep'), may hold values from 0 to 7, all different within a row; in each aligned block of 128 rows (0 to 127, 128 to 255, ...) at most 48 rows name the same one
- route_weight: float32 [4096, 2], P('ep'), may hold values from 0.2 to 1
- gate_weight: bfloat16 [8, 4096, 1024], P('ep', None, 'tp'), may hold values from -0.25 to 0.25
- up_weight: bfloat16 [8, 4096, 1024], P('ep', None, 'tp'), may hold values from -0.25 to 0.25
- down_weight: bfloat16 [8, 1024, 4096], P('ep', 'tp'), may hold values from -0.02734375 to 0.02734375
Outputs:
- mixed: bfloat16 [4096, 4096], P('ep', 'tp')
- expert_out: bfloat16 [4096, 4096], P(('ep', 'tp'))
Inputs may be any that keep to these rules, and one draw needn't show every extreme that they name: `routes`: each row names 2 different experts; within the rows of one device (aligned blocks of 128 rows) no expert is named more than 48 times, and that count is reached.
All inputs are finite; a program needn't handle non-finite values.
Results may differ from a plain program's by a relative error of at most 0.012.
Values may be sent and summed in bfloat16 or wider, within the bound.
A program may use at most 128 MiB of HBM per device.

v0:
```python
import jax
import jax.numpy as jnp
from jax import lax
from jax.sharding import PartitionSpec as P

WMAX = 16
CHUNKS = 3

epsilon = 1e-06
clamp_limit = 7.0
sigmoid_slope = 1.702


def from_behind(x, axis, by):
    count = lax.axis_size(axis)
    pairs = [(i, i + by) for i in range(count) if 0 <= i + by < count]
    return lax.ppermute(x, axis, pairs)


def rms_norm(values, gain):
    widened = values.astype(jnp.float32)
    scaled = widened * lax.rsqrt(jnp.mean(widened * widened, axis=-1, keepdims=True) + epsilon)
    return (scaled * gain).astype(jnp.bfloat16)


def clamped_unit(gate_part, up_part):
    gate_part = jnp.minimum(gate_part, clamp_limit)
    up_part = jnp.clip(up_part, -clamp_limit, clamp_limit)
    return ((up_part + 1.0) * gate_part * jax.nn.sigmoid(sigmoid_slope * gate_part)).astype(
        jnp.bfloat16
    )


def slot_ids(block_routes, experts, capacity):
    onehot = (
        block_routes[:, :, None] == jnp.arange(experts, dtype=jnp.int32)[None, None, :]
    ).astype(jnp.float32)
    per_token = jnp.sum(onehot, axis=1)
    count = block_routes.shape[0]
    before = (
        jnp.arange(count, dtype=jnp.int32)[:, None] > jnp.arange(count, dtype=jnp.int32)[None, :]
    ).astype(jnp.bfloat16)
    earlier = jnp.dot(before, per_token.astype(jnp.bfloat16), preferred_element_type=jnp.float32)
    rank = jnp.sum(onehot * earlier[:, None, :], axis=2).astype(jnp.int32)
    return block_routes, rank


def mixer_rows(mixer_in, mixer_gain):
    normed = rms_norm(mixer_in, mixer_gain)
    shard_rows = lax.all_to_all(normed, "tp", split_axis=1, concat_axis=0, tiled=True)
    length = shard_rows.shape[0]
    return shard_rows, from_behind(shard_rows[length - WMAX :], "ep", 1)


def mixer(shard_rows, before, group_weight, group_scale):
    length = shard_rows.shape[0]
    total = jnp.concatenate([before, shard_rows], axis=0).astype(jnp.float32)
    values = total[WMAX:]
    tp_index = lax.axis_index("tp")
    window = 2 << tp_index
    position = lax.axis_index("ep") * length + jnp.arange(length, dtype=jnp.int32)
    picked = jnp.zeros_like(values)
    reach = 1
    for level in range(lax.axis_size("tp")):
        total = total[reach:] + total[:-reach]
        reach = 2 * reach
        picked = jnp.where(tp_index == level, total[total.shape[0] - length :], picked)
    counts = jnp.minimum(position + 1, window).astype(jnp.float32)[:, None]
    pooled = (picked / counts - values).astype(jnp.bfloat16)
    return (
        jnp.dot(pooled, group_weight[0], preferred_element_type=jnp.float32) * group_scale[0]
    ).astype(jnp.bfloat16)


def shards(
    mixer_in,
    mixer_gain,
    group_weight,
    group_scale,
    expert_in,
    expert_gain,
    routes,
    route_weight,
    gate_weight,
    up_weight,
    down_weight,
):
    shard_rows, before = mixer_rows(mixer_in, mixer_gain)
    expert_in, shard_rows, before = lax.optimization_barrier((expert_in, shard_rows, before))
    mixed = mixer(shard_rows, before, group_weight, group_scale)
    expert_norm = rms_norm(expert_in, expert_gain)
    tok_count, width = expert_in.shape
    top = routes.shape[1]
    experts = lax.axis_size("ep")
    capacity = max(2, 3 * tok_count * top // (2 * experts))
    chunks = CHUNKS if capacity % CHUNKS == 0 else 1
    part = capacity // chunks
    tp_index = lax.axis_index("tp")
    own_routes = lax.dynamic_slice_in_dim(routes, tp_index * tok_count, tok_count, 0)
    own_weight = lax.dynamic_slice_in_dim(route_weight, tp_index * tok_count, tok_count, 0)
    gate_local = gate_weight[0]
    up_local = up_weight[0]
    down_full = lax.all_gather(down_weight[0], "tp", axis=0, tiled=True)
    expert_of, rank = slot_ids(own_routes, experts, capacity)
    expert_sum = jnp.zeros((tok_count, width), jnp.float32)
    pieces = []
    picks = []
    for chunk in range(chunks):
        inside = (rank >= chunk * part) & (rank < (chunk + 1) * part)
        slot = jnp.where(inside, expert_of * part + rank - chunk * part, -1)
        match = slot[:, :, None] == jnp.arange(experts * part, dtype=jnp.int32)[None, None, :]
        picks.append(match)
        pick = jnp.any(match, axis=1).astype(jnp.bfloat16)
        outgoing = lax.dot_general(
            pick, expert_norm, (((0,), (0,)), ((), ())), preferred_element_type=jnp.float32
        ).astype(jnp.bfloat16)
        if chunk > 0:
            outgoing, arrived = lax.optimization_barrier((outgoing, arrived))
        arrived = lax.all_to_all(outgoing, "ep", split_axis=0, concat_axis=0, tiled=True)
        if chunk == 1:
            arrived, down_full = lax.optimization_barrier((arrived, down_full))
        pieces.append(lax.all_gather(arrived, "tp", axis=0, tiled=True))
    for chunk in range(chunks):
        piece = pieces[chunk]
        if chunk > 0:
            piece, result = lax.optimization_barrier((piece, result))
        hidden = clamped_unit(
            jnp.dot(piece, gate_local, preferred_element_type=jnp.float32),
            jnp.dot(piece, up_local, preferred_element_type=jnp.float32),
        )
        hidden = lax.all_to_all(hidden, "tp", split_axis=0, concat_axis=1, tiled=True)
        result = jnp.dot(hidden, down_full, preferred_element_type=jnp.float32).astype(jnp.bfloat16)
        returned = lax.all_to_all(result, "ep", split_axis=0, concat_axis=0, tiled=True)
        weights = jnp.sum(jnp.where(picks[chunk], own_weight[:, :, None], 0.0), axis=1)
        high = weights.astype(jnp.bfloat16)
        low = (weights - high.astype(jnp.float32)).astype(jnp.bfloat16)
        expert_sum = (
            expert_sum
            + jnp.dot(high, returned, preferred_element_type=jnp.float32)
            + jnp.dot(low, returned, preferred_element_type=jnp.float32)
        )
    return (mixed, expert_sum.astype(jnp.bfloat16))


def solution(mesh):
    in_specs = (
        P(("ep", "tp"), None),
        P(),
        P("tp", None, None),
        P("tp", None),
        P(("ep", "tp"), None),
        P(),
        P("ep", None),
        P("ep", None),
        P("ep", None, "tp"),
        P("ep", None, "tp"),
        P("ep", "tp", None),
    )
    out_specs = (P("ep", "tp"), P(("ep", "tp"), None))
    return jax.shard_map(shards, mesh=mesh, in_specs=in_specs, out_specs=out_specs, check_vma=False)
```

profile of v0, /device:TPU:16, one launch (start us, length us, event | category | flops | bytes accessed | tf_op | source)
XLA Modules:
  0.0 283.9 jit_solution(611450616829126164)
XLA Ops:
  7.2 0.7 all-gather.12.cloned.1.call-update
  7.9 1.6 copy.39
  10.1 1.5 fusion.3
  11.6 4.4 %all-to-all-start = ((bf16[128,4,1024]{0,2,1:T(8,128)(2,1)}), bf16[128,4,1024]{0,2,1:T(8,128)(2,1)}, u32[]{:S(2)}, u32[]{:S(2)}) async-start(bf16[128,4,1024]{0,2,1:T(8,128)(2,1)} %bitcast.115), calls=%async_computation | async-start | bytes 2097152 | tf_op jit(solution)/shard_map/all_to_all | solution.py:50
  16.3 22.9 %all-to-all-done = bf16[128,4,1024]{0,2,1:T(8,128)(2,1)} async-done(((bf16[128,4,1024]{0,2,1:T(8,128)(2,1)}), bf16[128,4,1024]{0,2,1:T(8,128)(2,1)}, u32[]{:S(2)}, u32[]{:S(2)}) %all-to-all-start) | async-done | bytes 1048608 | tf_op jit(solution)/shard_map/all_to_all | solution.py:50
  39.2 2.3 copy.40
  41.5 0.8 slice.56
  42.3 3.5 %collective-permute-start = (bf16[16,1024]{1,0:T(8,128)(2,1)S(1)}, bf16[16,1024]{1,0:T(8,128)(2,1)}, u32[]{:S(2)}, u32[]{:S(2)}) collective-permute-start(bf16[16,1024]{1,0:T(8,128)(2,1)S(1)} %slice.56), channel_id=1, source_target_pairs={{0,4},{4,8},{8,12},{12,16},{16,20},{20,24},{24,28},{1,5},{5,9},{9,... | collective-permute-start | bytes 98312 | tf_op jit(solution)/shard_map/ppermute | solution.py:17
  45.9 3.2 %collective-permute-done = bf16[16,1024]{1,0:T(8,128)(2,1)} collective-permute-done((bf16[16,1024]{1,0:T(8,128)(2,1)S(1)}, bf16[16,1024]{1,0:T(8,128)(2,1)}, u32[]{:S(2)}, u32[]{:S(2)}) %collective-permute-start) | collective-permute-done | bytes 32800 | tf_op jit(solution)/shard_map/ppermute | solution.py:17
  49.9 26.9 %all_to_all.148 = bf16[8,16,4096]{2,1,0:T(8,128)(2,1)} all-to-all(bf16[8,16,4096]{2,1,0:T(8,128)(2,1)S(1)} %bitcast.117), channel_id=1, replica_groups=mesh['ep'=8,'tp'=4] {'ep'}, dimensions={0} | all-to-all | bytes 2097152 | tf_op jit(solution)/shard_map/all_to_all | solution.py:119
  77.5 28.0 %all_to_all.149 = bf16[8,16,4096]{2,1,0:T(8,128)(2,1)} all-to-all(bf16[8,16,4096]{2,1,0:T(8,128)(2,1)S(1)} %bitcast.118), channel_id=1, replica_groups=mesh['ep'=8,'tp'=4] {'ep'}, dimensions={0} | all-to-all | bytes 2097152 | tf_op jit(solution)/shard_map/all_to_all | solution.py:119
  106.1 28.8 %all_to_all.150 = bf16[8,16,4096]{2,1,0:T(8,128)(2,1)} all-to-all(bf16[8,16,4096]{2,1,0:T(8,128)(2,1)S(1)} %bitcast.116), channel_id=1, replica_groups=mesh['ep'=8,'tp'=4] {'ep'}, dimensions={0} | all-to-all | bytes 2097152 | tf_op jit(solution)/shard_map/all_to_all | solution.py:119
  135.1 4.3 %fusion.28 = f32[512,256]{1,0:T(8,128)S(1)} fusion(bf16[512,4096]{1,0:T(8,128)(2,1)} %all-gather.6.cloned.1.call-done, bf16[1,4096,256]{2,1,0:T(8,128)(2,1)} %param.19), kind=kOutput, calls=%fused_computation.48 | convolution fusion | flops 1073872896 | bytes 6815744 | tf_op jit(solution)/shard_map/dot_general | solution.py:128
  139.8 1.3 fusion.73
  141.3 9.3 %all_to_all.151 = bf16[4,128,256]{1,2,0:T(8,128)(2,1)S(1)} all-to-all(bf16[4,128,256]{1,2,0:T(8,128)(2,1)S(1)} %copy.41), channel_id=1, replica_groups=mesh['ep'=8,'tp'=4] {'tp'}, dimensions={0} | all-to-all | bytes 524288 | tf_op jit(solution)/shard_map/all_to_all | solution.py:131
  150.6 5.6 %convolution_convert_fusion.3 = bf16[128,4096]{1,0:T(8,128)(2,1)} fusion(bf16[128,1024]{0,1:T(8,128)(2,1)S(1)} %bitcast.127, bf16[1024,4096]{1,0:T(8,128)(2,1)} %bitcast.106), kind=kOutput, calls=%fused_computation.9 | convolution fusion | flops 1074266112 | bytes 9699328 | tf_op jit(solution)/shard_map/dot_general | solution.py:132
  156.2 4.5 %fusion.31 = f32[512,256]{1,0:T(8,128)S(1)} fusion(bf16[512,4096]{1,0:T(8,128)(2,1)} %all-gather.8.cloned.1.call-done, bf16[1,4096,256]{2,1,0:T(8,128)(2,1)} %param.19), kind=kOutput, calls=%fused_computation.49 | convolution fusion | flops 1073872896 | bytes 6815744 | tf_op jit(solution)/shard_map/dot_general | solution.py:128
  160.9 0.8 copy-done.13
  161.8 1.3 fusion.76
  163.2 11.6 %all_to_all.152 = bf16[4,128,256]{1,2,0:T(8,128)(2,1)S(1)} all-to-all(bf16[4,128,256]{1,2,0:T(8,128)(2,1)S(1)} %copy.42), channel_id=1, replica_groups=mesh['ep'=8,'tp'=4] {'tp'}, dimensions={0} | all-to-all | bytes 524288 | tf_op jit(solution)/shard_map/all_to_all | solution.py:131
  174.8 6.0 %all-to-all-start.4 = ((bf16[8,16,4096]{2,1,0:T(8,128)(2,1)}), bf16[8,16,4096]{2,1,0:T(8,128)(2,1)S(1)}, u32[]{:S(2)}, u32[]{:S(2)}) async-start(bf16[8,16,4096]{2,1,0:T(8,128)(2,1)} %bitcast.123), calls=%async_computation.4 | async-start | bytes 2097152 | tf_op jit(solution)/shard_map/all_to_all | solution.py:133
  180.9 0.7 constant_dynamic-slice_fusion
  181.5 0.8 select_reduce_fusion
  182.4 5.7 %convolution_convert_fusion.2 = bf16[128,4096]{1,0:T(8,128)(2,1)} fusion(bf16[128,1024]{0,1:T(8,128)(2,1)S(1)} %bitcast.126, bf16[1024,4096]{1,0:T(8,128)(2,1)} %bitcast.107), kind=kOutput, calls=%fused_computation.8 | convolution fusion | flops 1074266112 | bytes 9699328 | tf_op jit(solution)/shard_map/dot_general | solution.py:132
  188.1 1.3 all-gather.10.cloned.1.call-done
  189.4 4.3 %fusion.34 = f32[512,256]{1,0:T(8,128)S(1)} fusion(bf16[512,4096]{1,0:T(8,128)(2,1)} %all-gather.10.cloned.1.call-done, bf16[1,4096,256]{2,1,0:T(8,128)(2,1)} %param.19), kind=kOutput, calls=%fused_computation.50 | convolution fusion | flops 1073872896 | bytes 6815744 | tf_op jit(solution)/shard_map/dot_general | solution.py:128
  194.2 1.3 fusion.79
  195.4 0.8 copy.43
  196.3 7.0 %all-to-all-done.4 = bf16[8,16,4096]{2,1,0:T(8,128)(2,1)S(1)} async-done(((bf16[8,16,4096]{2,1,0:T(8,128)(2,1)}), bf16[8,16,4096]{2,1,0:T(8,128)(2,1)S(1)}, u32[]{:S(2)}, u32[]{:S(2)}) %all-to-all-start.4) | async-done | bytes 1048608 | tf_op jit(solution)/shard_map/all_to_all | solution.py:133
  203.3 3.4 %all-to-all-start.8 = ((bf16[4,128,256]{1,2,0:T(8,128)(2,1)}), bf16[4,128,256]{1,2,0:T(8,128)(2,1)S(1)}, u32[]{:S(2)}, u32[]{:S(2)}) async-start(bf16[4,128,256]{1,2,0:T(8,128)(2,1)} %copy.43), calls=%async_computation.8 | async-start | bytes 524288 | tf_op jit(solution)/shard_map/all_to_all | solution.py:131
  206.7 2.9 %maximum_convert_fusion = f32[528,1024]{1,0:T(8,128)} fusion(bf16[512,1024]{1,0:T(8,128)(2,1)} %bitcast.114, bf16[16,1024]{1,0:T(8,128)(2,1)} %collective-permute-done), kind=kLoop, calls=%fused_computation.66 | loop fusion | flops 2162688 | bytes 3244032 | tf_op jit(solution)/shard_map/convert_element_type | solution.py:57
  209.6 3.0 %all-to-all-done.8 = bf16[4,128,256]{1,2,0:T(8,128)(2,1)S(1)} async-done(((bf16[4,128,256]{1,2,0:T(8,128)(2,1)}), bf16[4,128,256]{1,2,0:T(8,128)(2,1)S(1)}, u32[]{:S(2)}, u32[]{:S(2)}) %all-to-all-start.8) | async-done | bytes 262176 | tf_op jit(solution)/shard_map/all_to_all | solution.py:131
  212.7 7.4 %all-to-all-start.6 = ((bf16[8,16,4096]{2,1,0:T(8,128)(2,1)}), bf16[8,16,4096]{2,1,0:T(8,128)(2,1)}, u32[]{:S(2)}, u32[]{:S(2)}) async-start(bf16[8,16,4096]{2,1,0:T(8,128)(2,1)} %bitcast.122), calls=%async_computation.6 | async-start | bytes 2097152 | tf_op jit(solution)/shard_map/all_to_all | solution.py:133
  220.1 2.7 slice_add_fusion.2
  223.1 1.1 copy-done.1
  224.7 0.9 copy-done.2
  225.5 2.6 fusion.99
  228.2 0.6 copy-done.3
  228.7 1.4 slice-done.1
  230.1 2.3 convolution_convert_fusion
  232.4 10.2 %all-to-all-done.6 = bf16[8,16,4096]{2,1,0:T(8,128)(2,1)} async-done(((bf16[8,16,4096]{2,1,0:T(8,128)(2,1)}), bf16[8,16,4096]{2,1,0:T(8,128)(2,1)}, u32[]{:S(2)}, u32[]{:S(2)}) %all-to-all-start.6) | async-done | bytes 1048608 | tf_op jit(solution)/shard_map/all_to_all | solution.py:133
  242.6 7.5 %all-to-all-start.9 = ((bf16[8,16,4096]{2,1,0:T(8,128)(2,1)}), bf16[8,16,4096]{2,1,0:T(8,128)(2,1)}, u32[]{:S(2)}, u32[]{:S(2)}) async-start(bf16[8,16,4096]{2,1,0:T(8,128)(2,1)} %bitcast.124), calls=%async_computation.9 | async-start | bytes 2097152 | tf_op jit(solution)/shard_map/all_to_all | solution.py:133
  250.1 7.7 %multiply_convert_fusion = bf16[512,1024]{1,0:T(8,128)(2,1)} fusion(bf16[1,1024,1024]{2,1,0:T(8,128)(2,1)S(1)} %copy-done, f32[1024]{0:T(1024)S(1)} %bitcast.131, f32[528,1024]{1,0:T(8,128)} %maximum_convert_fusion, f32[527,1024]{1,0:T(8,128)} %copy-done.1, f32[525,1024]{1,0:T(8,128)} %copy-done.2, f32[521,1024]{1,0:T(8,128)} %copy-done.3, ...), kind=kOutput, calls=%fused_computation.47 | convolution fusion | flops 1078984704 | bytes 15734788 | tf_op jit(solution)/shard_map/dot_general | solution.py:71
  259.0 1.6 convolution_add_fusion.3
  260.7 3.0 %convolution_add_fusion.2 = f32[128,4096]{1,0:T(8,128)} fusion(f32[128,4096]{1,0:T(8,128)S(1)} %convolution_add_fusion.3, bf16[128,4096]{1,0:T(8,128)(2,1)} %bitcast.21, f32[128,128]{1,0:T(8,128)S(1)} %copy-done.5), kind=kOutput, calls=%fused_computation.2 | convolution fusion | flops 134807552 | bytes 5308416 | tf_op jit(solution)/shard_map/dot_general | solution.py:140
  263.7 8.7 %all-to-all-done.9 = bf16[8,16,4096]{2,1,0:T(8,128)(2,1)} async-done(((bf16[8,16,4096]{2,1,0:T(8,128)(2,1)}), bf16[8,16,4096]{2,1,0:T(8,128)(2,1)}, u32[]{:S(2)}, u32[]{:S(2)}) %all-to-all-start.9) | async-done | bytes 1048608 | tf_op jit(solution)/shard_map/all_to_all | solution.py:133
  272.4 2.3 convolution_add_fusion.1
  274.7 2.6 fusion
  (63 shorter events, 6.6 us)
Async XLA Ops:
  7.2 242.9 %copy-start = (bf16[1,1024,1024]{2,1,0:T(8,128)(2,1)S(1)}, bf16[1,1024,1024]{2,1,0:T(8,128)(2,1)}, u32[]{:S(2)}) copy-start(bf16[1,1024,1024]{2,1,0:T(8,128)(2,1)} %param.13) | copy-start | bytes 6291460
  7.2 98.4 %all-gather.12.cloned.1.call-start = ((), (), s32[]{:S(2)}) async-start(), calls=%async_computation.13 | async-start | bytes 10485760 | tf_op jit(solution)/shard_map/all_gather | solution.py:103
  7.9 2.2 copy-start.7
  10.1 6.0 %copy-start.8 = (s32[512,2]{0,1:T(2,128)S(1)}, s32[512,2]{0,1:T(2,128)}, u32[]{:S(2)}) copy-start(s32[512,2]{0,1:T(2,128)} %param.17) | copy-start | bytes 12292
  11.6 37.4 %copy-start.4 = (bf16[128,4096]{1,0:T(8,128)(2,1)S(1)}, bf16[128,4096]{1,0:T(8,128)(2,1)}, u32[]{:S(2)}) copy-start(bf16[128,4096]{1,0:T(8,128)(2,1)} %param.15) | copy-start | bytes 3145732
  11.6 27.6 %all-to-all-start = ((bf16[128,4,1024]{0,2,1:T(8,128)(2,1)}), bf16[128,4,1024]{0,2,1:T(8,128)(2,1)}, u32[]{:S(2)}, u32[]{:S(2)}) async-start(bf16[128,4,1024]{0,2,1:T(8,128)(2,1)} %bitcast.115), calls=%async_computation | async-start | bytes 2097152 | tf_op jit(solution)/shard_map/all_to_all | solution.py:50
  16.0 33.4 %copy-start.6 = (f32[4096]{0:T(1024)S(1)}, f32[4096]{0:T(1024)}, u32[]{:S(2)}) copy-start(f32[4096]{0:T(1024)} %param.16) | copy-start | bytes 49156
  16.0 119.0 %all-gather.6.cloned.1.call-start = ((), (), s32[]{:S(2)}) async-start(), calls=%async_computation.10 | async-start | bytes 5242880 | tf_op jit(solution)/shard_map/all_gather | solution.py:122
  42.3 6.8 %collective-permute-start = (bf16[16,1024]{1,0:T(8,128)(2,1)S(1)}, bf16[16,1024]{1,0:T(8,128)(2,1)}, u32[]{:S(2)}, u32[]{:S(2)}) collective-permute-start(bf16[16,1024]{1,0:T(8,128)(2,1)S(1)} %slice.56), channel_id=1, source_target_pairs={{0,4},{4,8},{8,12},{12,16},{16,20},{20,24},{24,28},{1,5},{5,9},{9,... | collective-permute-start | bytes 98312 | tf_op jit(solution)/shard_map/ppermute | solution.py:17
  76.9 79.4 %all-gather.8.cloned.1.call-start = ((), (), s32[]{:S(2)}) async-start(), calls=%async_computation.11 | async-start | bytes 5242880 | tf_op jit(solution)/shard_map/all_gather | solution.py:122
  105.6 83.9 %all-gather.10.cloned.1.call-start = ((), (), s32[]{:S(2)}) async-start(), calls=%async_computation.12 | async-start | bytes 5242880 | tf_op jit(solution)/shard_map/all_gather | solution.py:122
  135.0 4.3 %copy-start.10 = (bf16[512,4096]{1,0:T(8,128)(2,1)S(1)}, bf16[512,4096]{1,0:T(8,128)(2,1)}, u32[]{:S(2)}) copy-start(bf16[512,4096]{1,0:T(8,128)(2,1)} %all-gather.6.cloned.1.call-done) | copy-start | bytes 12582916
  135.0 4.8 %copy-start.12 = (bf16[1,4096,256]{2,1,0:T(8,128)(2,1)S(1)}, bf16[1,4096,256]{2,1,0:T(8,128)(2,1)}, u32[]{:S(2)}) copy-start(bf16[1,4096,256]{2,1,0:T(8,128)(2,1)} %param.20) | copy-start | bytes 6291460
  156.2 4.7 %copy-start.11 = (bf16[512,4096]{1,0:T(8,128)(2,1)S(1)}, bf16[512,4096]{1,0:T(8,128)(2,1)}, u32[]{:S(2)}) copy-start(bf16[512,4096]{1,0:T(8,128)(2,1)} %all-gather.8.cloned.1.call-done) | copy-start | bytes 12582916
  156.2 5.5 %copy-start.13 = (bf16[1,4096,256]{2,1,0:T(8,128)(2,1)S(1)}, bf16[1,4096,256]{2,1,0:T(8,128)(2,1)}, u32[]{:S(2)}) copy-start(bf16[1,4096,256]{2,1,0:T(8,128)(2,1)} %param.20) | copy-start | bytes 6291460
  174.8 28.5 %all-to-all-start.4 = ((bf16[8,16,4096]{2,1,0:T(8,128)(2,1)}), bf16[8,16,4096]{2,1,0:T(8,128)(2,1)S(1)}, u32[]{:S(2)}, u32[]{:S(2)}) async-start(bf16[8,16,4096]{2,1,0:T(8,128)(2,1)} %bitcast.123), calls=%async_computation.4 | async-start | bytes 2097152 | tf_op jit(solution)/shard_map/all_to_all | solution.py:133
  189.4 4.3 %copy-start.9 = (bf16[512,4096]{1,0:T(8,128)(2,1)S(1)}, bf16[512,4096]{1,0:T(8,128)(2,1)}, u32[]{:S(2)}) copy-start(bf16[512,4096]{1,0:T(8,128)(2,1)} %all-gather.10.cloned.1.call-done) | copy-start | bytes 12582916
  189.4 4.7 %copy-start.14 = (bf16[1,4096,256]{2,1,0:T(8,128)(2,1)S(1)}, bf16[1,4096,256]{2,1,0:T(8,128)(2,1)}, u32[]{:S(2)}) copy-start(bf16[1,4096,256]{2,1,0:T(8,128)(2,1)} %param.20) | copy-start | bytes 6291460
  203.3 9.4 %all-to-all-start.8 = ((bf16[4,128,256]{1,2,0:T(8,128)(2,1)}), bf16[4,128,256]{1,2,0:T(8,128)(2,1)S(1)}, u32[]{:S(2)}, u32[]{:S(2)}) async-start(bf16[4,128,256]{1,2,0:T(8,128)(2,1)} %copy.43), calls=%async_computation.8 | async-start | bytes 524288 | tf_op jit(solution)/shard_map/all_to_all | solution.py:131
  212.7 29.9 %all-to-all-start.6 = ((bf16[8,16,4096]{2,1,0:T(8,128)(2,1)}), bf16[8,16,4096]{2,1,0:T(8,128)(2,1)}, u32[]{:S(2)}, u32[]{:S(2)}) async-start(bf16[8,16,4096]{2,1,0:T(8,128)(2,1)} %bitcast.122), calls=%async_computation.6 | async-start | bytes 2097152 | tf_op jit(solution)/shard_map/all_to_all | solution.py:133
  222.8 1.4 copy-start.1
  222.8 5.9 %slice-start = ((s8[8388608]{0:T(1024)(128)(4,1)}), s8[4194304]{0:T(1024)(128)(4,1)S(1)}, s32[]{:S(2)}) async-start(s8[8388608]{0:T(1024)(128)(4,1)} %bitcast.108), calls=%async_computation.14 | async-start | bytes 8388608
  224.2 1.3 copy-start.2
  224.2 5.9 %slice-start.1 = ((s8[8388608]{0:T(1024)(128)(4,1)}), s8[4194304]{0:T(1024)(128)(4,1)S(1)}, s32[]{:S(2)}) async-start(s8[8388608]{0:T(1024)(128)(4,1)} %bitcast.108), calls=%async_computation.15 | async-start | bytes 8388608
  225.5 3.2 %copy-start.3 = (f32[521,1024]{1,0:T(8,128)}, f32[521,1024]{1,0:T(8,128)S(1)}, u32[]{:S(2)}) copy-start(f32[521,1024]{1,0:T(8,128)S(1)} %slice_add_fusion) | copy-start | bytes 6402052
  232.4 17.7 %copy-start.15 = (f32[1,1024]{1,0:T(1,128)S(1)}, f32[1,1024]{1,0:T(1,128)}, u32[]{:S(2)}) copy-start(f32[1,1024]{1,0:T(1,128)} %param.14) | copy-start | bytes 12292
  242.6 29.8 %all-to-all-start.9 = ((bf16[8,16,4096]{2,1,0:T(8,128)(2,1)}), bf16[8,16,4096]{2,1,0:T(8,128)(2,1)}, u32[]{:S(2)}, u32[]{:S(2)}) async-start(bf16[8,16,4096]{2,1,0:T(8,128)(2,1)} %bitcast.124), calls=%async_computation.9 | async-start | bytes 2097152 | tf_op jit(solution)/shard_map/all_to_all | solution.py:133
  258.2 0.8 copy-start.5
Sparse Core Ops, SparseCore 0:
  9.5 67.5 all-gather.11
  78.7 34.5 all-gather.5
  114.9 34.8 all-gather.7
  151.2 38.2 all-gather.9
where the time goes:
time: 289 us; the launch traced here: 284 us
  blocking collectives  105 us (36%)
  waiting for transfers between devices  57.2 us (20%)
  matrix products  50.2 us (17%)
  starting transfers between devices  32.4 us (11%)
  local copies, waits for them, and re-layouts  15.4 us (5%)
  between operations  14.1 us (5%)
  other arithmetic  9.82 us (3%)
    all_to_all x3, blocking collectives, shards(): lax.all_to_all(outgoing, 'ep', split_axis=0, concat_axis=0, tiled=True)  83.7 us
    all_to_all x3, waiting for transfers between devices, shards(): lax.all_to_all(result, 'ep', split_axis=0, concat_axis=0, tiled=True)  26 us
    all_to_all x1, waiting for transfers between devices, mixer_rows(): lax.all_to_all(normed, 'tp', split_axis=1, concat_axis=0, tiled=True)  22.9 us
    all_to_all x3, starting transfers between devices, shards(): lax.all_to_all(result, 'ep', split_axis=0, concat_axis=0, tiled=True)  21 us
    all_to_all x2, blocking collectives, shards(): lax.all_to_all(hidden, 'tp', split_axis=0, concat_axis=1, tiled=True)  20.9 us
    dot_general x3, matrix products, shards(): jnp.dot(hidden, down_full, preferred_element_type=jnp.float32)  13.6 us
    dot_general x3, matrix products, shards(): jnp.dot(piece, gate_local, preferred_element_type=jnp.float32)  13 us
    unnamed x37, local copies, waits for them, and re-layouts  7.92 us
  transfers between devices with their start and end apart: 10, of which 7 were waited for; matrix products, arithmetic and copies ran while one was open for 23% of the time, Pallas kernels for 0%

commit v1 on v0

v1 whole, which is shorter than its diff:
```python
import functools
import jax
import jax.numpy as jnp
from jax import lax
from jax.experimental import pallas as pl
from jax.experimental.pallas import tpu as pltpu
from jax.sharding import PartitionSpec as P

WMAX = 16
NORM_ROWS = 16
K_CHUNKS = 8
D_CHUNKS = 8

epsilon = 1e-06
clamp_limit = 7.0
sigmoid_slope = 1.702

MESH = pl.DeviceIdType.MESH


def clamped_unit(gate_part, up_part):
    gate_part = jnp.minimum(gate_part, clamp_limit)
    up_part = jnp.clip(up_part, -clamp_limit, clamp_limit)
    return ((up_part + 1.0) * gate_part * jax.nn.sigmoid(sigmoid_slope * gate_part)).astype(
        jnp.bfloat16
    )


def norm_rows(source, gain, at):
    widened = source[pl.ds(at, NORM_ROWS), :].astype(jnp.float32)
    mean = jnp.sum(widened * widened, axis=-1, keepdims=True) * (1.0 / widened.shape[-1])
    return (widened * lax.rsqrt(mean + epsilon) * gain[...]).astype(jnp.bfloat16)


def aligned(value, size):
    return pl.multiple_of(value * size, size)


def kernel(
    n_ep,
    n_tp,
    mixer_in,
    mixer_gain,
    group_weight,
    group_scale,
    expert_in,
    expert_gain,
    routes,
    route_weight,
    gate_w,
    up_w,
    down_w,
    mixed_out,
    expert_out,
    x_in,
    m_in,
    e_gain,
    m_gain,
    scale,
    named,
    shares,
    gate_b,
    up_b,
    down_b,
    normed,
    pick,
    share_high,
    share_low,
    outgoing,
    arrived,
    acc_gate,
    acc_up,
    hidden,
    result,
    returned,
    m_normed,
    m_rows,
    g_weight,
    m_out,
    e_out,
    load_sem,
    gate_send,
    gate_recv,
    up_send,
    up_recv,
    down_send,
    down_recv,
    out_send,
    out_recv,
    ret_send,
    ret_recv,
    mix_send,
    mix_recv,
    halo_send,
    halo_recv,
    m_store,
    e_store,
):
    ep = lax.axis_index("ep")
    tp = lax.axis_index("tp")
    tokens, width = x_in.shape
    group_width = g_weight.shape[0]
    slots, units = hidden.shape
    capacity = arrived.shape[1]
    part_units = units // n_tp
    k_size = width // K_CHUNKS
    d_size = width // D_CHUNKS

    def peer(i):
        return lax.rem(ep + i, n_ep)

    loads = [
        pltpu.make_async_copy(source, target, load_sem.at[i])
        for i, (source, target) in enumerate(
            [
                (expert_in, x_in),
                (expert_gain, e_gain),
                (routes, named),
                (route_weight, shares),
                (mixer_in, m_in),
                (mixer_gain, m_gain),
                (group_scale, scale),
                (group_weight.at[0], g_weight),
            ]
        )
    ]
    for load in loads:
        load.start()

    barrier = pltpu.get_barrier_semaphore()
    for r in range(1, n_tp):
        pl.semaphore_signal(barrier, inc=1, device_id={"tp": tp ^ r}, device_id_type=MESH)

    @pl.loop(1, n_ep)
    def _(i):
        pl.semaphore_signal(barrier, inc=1, device_id={"ep": peer(i)}, device_id_type=MESH)

    def weight_copy(kind, r, j):
        low = r & -r
        if kind == "down":
            source, target, send, recv = down_w, down_b, down_send, down_recv
            span = (slice(None), pl.ds(aligned(j, d_size), d_size))
        else:
            source, target = (gate_w, gate_b) if kind == "gate" else (up_w, up_b)
            send, recv = (gate_send, gate_recv) if kind == "gate" else (up_send, up_recv)
            span = (pl.ds(aligned(j, k_size), k_size), slice(None))
        origin = source.at[(0,) + span] if r == low else target.at[(r ^ low,) + span]
        if r == 0:
            return pltpu.make_async_copy(origin, target.at[(0,) + span], recv.at[0, j])
        return pltpu.make_async_remote_copy(
            src_ref=origin,
            dst_ref=target.at[(r,) + span],
            send_sem=send.at[r, j],
            recv_sem=recv.at[r, j],
            device_id={"tp": tp ^ low},
            device_id_type=MESH,
        )

    bits = []
    while (1 << len(bits)) < n_tp:
        bits.insert(0, 1 << len(bits))
    own_targets = bits
    forwards = {r: [r | b for b in bits if b < (r & -r)] for r in range(1, n_tp)}
    order = [0] + sorted(range(1, n_tp), key=lambda r: (r & (n_tp // 2) > 0, bin(r).count("1")))

    @pl.loop(0, K_CHUNKS)
    def _(j):
        weight_copy("gate", 0, j).start()
        weight_copy("up", 0, j).start()

    pl.semaphore_wait(barrier, n_ep - 1 + n_tp - 1)

    for target in own_targets:

        @pl.loop(0, K_CHUNKS)
        def _(j):
            weight_copy("gate", target, j).start()
            weight_copy("up", target, j).start()

    for load in loads[:4]:
        load.wait()
    mine = pl.ds(aligned(tp, tokens), tokens)
    own = named[:, mine]
    own_share = shares[:, mine]
    top = own.shape[0]
    experts = lax.broadcasted_iota(jnp.int32, (n_ep, tokens), 0)
    onehot = [
        (experts == jnp.broadcast_to(own[k : k + 1, :], (n_ep, tokens))).astype(jnp.float32)
        for k in range(top)
    ]
    per_token = functools.reduce(lambda a, b: a + b, onehot)
    before = (
        lax.broadcasted_iota(jnp.int32, (tokens, tokens), 0)
        < lax.broadcasted_iota(jnp.int32, (tokens, tokens), 1)
    ).astype(jnp.bfloat16)
    earlier = jnp.dot(per_token.astype(jnp.bfloat16), before, preferred_element_type=jnp.float32)
    slot_rows = lax.broadcasted_iota(jnp.int32, (slots, tokens), 0)
    picked = jnp.zeros((slots, tokens), jnp.float32)
    spread = jnp.zeros((slots, tokens), jnp.float32)
    for k in range(top):
        rank = jnp.sum(onehot[k] * earlier, axis=0, keepdims=True).astype(jnp.int32)
        slot = own[k : k + 1, :] * capacity + rank
        match = slot_rows == jnp.broadcast_to(slot, (slots, tokens))
        picked = picked + jnp.where(match, 1.0, 0.0)
        spread = spread + jnp.where(
            match, jnp.broadcast_to(own_share[k : k + 1, :], (slots, tokens)), 0.0
        )
    pick[...] = picked.reshape(n_ep, capacity, tokens).astype(jnp.bfloat16)
    spread = spread.T
    high = spread.astype(jnp.bfloat16)
    share_high[...] = high
    share_low[...] = (spread - high.astype(jnp.float32)).astype(jnp.bfloat16)

    @pl.loop(0, tokens // NORM_ROWS)
    def _(i):
        at = aligned(i, NORM_ROWS)
        normed[pl.ds(at, NORM_ROWS), :] = norm_rows(x_in, e_gain, at)

    def send_rows(i):
        return pltpu.make_async_remote_copy(
            src_ref=outgoing.at[peer(i)],
            dst_ref=arrived.at[ep],
            send_sem=out_send.at[i],
            recv_sem=out_recv.at[i],
            device_id={"ep": peer(i)},
            device_id_type=MESH,
        )

    @pl.loop(1, n_ep)
    def _(i):
        outgoing[peer(i)] = jnp.dot(
            pick[peer(i)], normed[...], preferred_element_type=jnp.float32
        ).astype(jnp.bfloat16)
        send_rows(i).start()

    arrived[ep] = jnp.dot(pick[ep], normed[...], preferred_element_type=jnp.float32).astype(
        jnp.bfloat16
    )

    @pl.loop(0, D_CHUNKS)
    def _(j):
        weight_copy("down", 0, j).start()

    for target in own_targets:

        @pl.loop(0, D_CHUNKS)
        def _(j):
            weight_copy("down", target, j).start()

    for load in loads[4:]:
        load.wait()

    @pl.loop(0, tokens // NORM_ROWS)
    def _(i):
        at = aligned(i, NORM_ROWS)
        rows = norm_rows(m_in, m_gain, at)
        for g in range(n_tp):
            m_normed[g, pl.ds(at, NORM_ROWS), :] = rows[:, g * group_width : (g + 1) * group_width]

    own_rows = pl.ds(pl.multiple_of(WMAX + tp * tokens, WMAX), tokens)

    def send_mix(r):
        return pltpu.make_async_remote_copy(
            src_ref=m_normed.at[tp ^ r],
            dst_ref=m_rows.at[own_rows, :],
            send_sem=mix_send.at[r],
            recv_sem=mix_recv.at[r],
            device_id={"tp": tp ^ r},
            device_id_type=MESH,
        )

    for r in range(1, n_tp):
        send_mix(r).start()
    m_rows[own_rows, :] = m_normed[tp]

    half = n_tp // 2
    early = K_CHUNKS - 2

    def forward(kind, r, j):
        if forwards[r]:
            weight_copy(kind, r, j).wait_recv()
            for target in forwards[r]:
                weight_copy(kind, target, j).start()

    def forward_all(kinds, j):
        for r in order[1:]:
            for kind in kinds:
                forward(kind, r, j)

    def arrive(kinds, r, j):
        if r == 0:
            for kind in kinds:
                weight_copy(kind, 0, j).wait()
        elif not forwards[r]:
            for kind in kinds:
                weight_copy(kind, r, j).wait_recv()

    def accumulate(r, j, first):
        rows = arrived[:, :, pl.ds(aligned(j, k_size), k_size)].reshape(slots, k_size)
        span = pl.ds(aligned(j, k_size), k_size)
        for acc, weight in ((acc_gate, gate_b), (acc_up, up_b)):
            product = jnp.dot(rows, weight[r, span, :], preferred_element_type=jnp.float32)
            if first:
                acc[r] = product
            else:
                acc[r] += product

    both = ("gate", "up")

    @pl.loop(0, early)
    def _(j):
        forward_all(both, j)

    @pl.loop(1, n_ep)
    def _(i):
        pltpu.make_async_remote_copy(
            src_ref=outgoing.at[peer(i)],
            dst_ref=arrived.at[lax.rem(ep + n_ep - i, n_ep)],
            send_sem=out_send.at[i],
            recv_sem=out_recv.at[i],
            device_id={"ep": peer(i)},
            device_id_type=MESH,
        ).wait_recv()

    def chunk(j, first, forwarding):
        if forwarding:
            forward_all(both, j)
        for r in order:
            arrive(both, r, j)
            accumulate(r, j, first)

    chunk(0, True, False)

    @pl.loop(1, early)
    def _(j):
        chunk(j, False, False)

    @pl.loop(early, K_CHUNKS)
    def _(j):
        chunk(j, False, True)

    for r in range(n_tp):
        hidden[:, r * part_units : (r + 1) * part_units] = clamped_unit(acc_gate[r], acc_up[r])

    def send_back(j, i):
        return pltpu.make_async_remote_copy(
            src_ref=result.at[j, peer(i)],
            dst_ref=returned.at[j, ep],
            send_sem=ret_send.at[j, i],
            recv_sem=ret_recv.at[j, i],
            device_id={"ep": peer(i)},
            device_id_type=MESH,
        )

    @pl.loop(0, D_CHUNKS)
    def _(j):
        forward_all(("down",), j)
        for r in order:
            arrive(("down",), r, j)
        weight = down_b[:, :, pl.ds(aligned(j, d_size), d_size)].reshape(units, d_size)
        product = jnp.dot(hidden[...], weight, preferred_element_type=jnp.float32)
        result[j] = product.astype(jnp.bfloat16).reshape(n_ep, capacity, d_size)

        @pl.loop(1, n_ep)
        def _(i):
            send_back(j, i).start()

        returned[j, ep] = result[j, ep]

    for r in range(1, n_tp):
        theirs = pl.ds(pl.multiple_of(WMAX + (tp ^ r) * tokens, WMAX), tokens)
        pltpu.make_async_remote_copy(
            src_ref=m_normed.at[tp ^ r],
            dst_ref=m_rows.at[theirs, :],
            send_sem=mix_send.at[r],
            recv_sem=mix_recv.at[r],
            device_id={"tp": tp ^ r},
            device_id_type=MESH,
        ).wait_recv()
    halo = pltpu.make_async_remote_copy(
        src_ref=m_rows.at[n_tp * tokens : n_tp * tokens + WMAX, :],
        dst_ref=m_rows.at[0:WMAX, :],
        send_sem=halo_send,
        recv_sem=halo_recv,
        device_id={"ep": peer(1)},
        device_id_type=MESH,
    )
    halo.start()
    halo.wait_recv()
    window = 2 << tp
    span_rows = tokens + WMAX
    here = lax.broadcasted_iota(jnp.int32, (tokens, span_rows), 0)
    there = lax.broadcasted_iota(jnp.int32, (tokens, span_rows), 1)
    back = here + WMAX - there
    inside = (back >= 0) & (back < window)
    row = lax.broadcasted_iota(jnp.int32, (tokens, 1), 0)
    stores = []
    for b in range(n_tp):
        position = (ep * n_tp + b) * tokens
        band = (inside & (there + position >= WMAX)).astype(jnp.bfloat16)
        values = m_rows[b * tokens : b * tokens + span_rows, :]
        total = jnp.dot(band, values, preferred_element_type=jnp.float32)
        counts = jnp.minimum(row + position + 1, window).astype(jnp.float32)
        pooled = (total / counts - values[WMAX:, :].astype(jnp.float32)).astype(jnp.bfloat16)
        product = jnp.dot(pooled, g_weight[...], preferred_element_type=jnp.float32)
        m_out[b] = (product * scale[...]).astype(jnp.bfloat16)
        store = pltpu.make_async_copy(
            m_out.at[b], mixed_out.at[b * tokens : (b + 1) * tokens, :], m_store.at[b]
        )
        store.start()
        stores.append(store)

    def write_out(j):
        return pltpu.make_async_copy(
            e_out.at[j], expert_out.at[:, pl.ds(aligned(j, d_size), d_size)], e_store.at[j]
        )

    @pl.loop(0, D_CHUNKS)
    def _(j):
        @pl.loop(1, n_ep)
        def _(i):
            pltpu.make_async_remote_copy(
                src_ref=result.at[j, peer(i)],
                dst_ref=returned.at[j, lax.rem(ep + n_ep - i, n_ep)],
                send_sem=ret_send.at[j, i],
                recv_sem=ret_recv.at[j, i],
                device_id={"ep": peer(i)},
                device_id_type=MESH,
            ).wait_recv()

        rows = returned[j].reshape(slots, d_size)
        e_out[j] = (
            jnp.dot(share_high[...], rows, preferred_element_type=jnp.float32)
            + jnp.dot(share_low[...], rows, preferred_element_type=jnp.float32)
        ).astype(jnp.bfloat16)
        write_out(j).start()

    for r in range(1, n_tp):

        @pl.loop(0, K_CHUNKS)
        def _(j):
            weight_copy("gate", r, j).wait_send()
            weight_copy("up", r, j).wait_send()

        @pl.loop(0, D_CHUNKS)
        def _(j):
            weight_copy("down", r, j).wait_send()

        send_mix(r).wait_send()
    halo.wait_send()

    @pl.loop(1, n_ep)
    def _(i):
        send_rows(i).wait_send()

    @pl.loop(0, D_CHUNKS)
    def _(j):
        @pl.loop(1, n_ep)
        def _(i):
            send_back(j, i).wait_send()

        write_out(j).wait()

    for store in stores:
        store.wait()


def shards(
    mixer_in,
    mixer_gain,
    group_weight,
    group_scale,
    expert_in,
    expert_gain,
    routes,
    route_weight,
    gate_weight,
    up_weight,
    down_weight,
):
    n_ep = lax.axis_size("ep")
    n_tp = lax.axis_size("tp")
    tokens, width = expert_in.shape
    group_width = group_weight.shape[-1]
    block_tokens, top = routes.shape
    part_units = gate_weight.shape[-1]
    units = part_units * n_tp
    capacity = max(2, 3 * tokens * top // (2 * n_ep))
    capacity = -(-capacity // 8) * 8
    slots = n_ep * capacity
    d_size = width // D_CHUNKS
    bf16, f32 = jnp.bfloat16, jnp.float32
    vmem = pltpu.VMEM
    dma = pltpu.SemaphoreType.DMA
    anywhere = pl.BlockSpec(memory_space=pl.ANY)
    scratch = [
        vmem((tokens, width), bf16),
        vmem((tokens, width), bf16),
        vmem((1, width), f32),
        vmem((1, width), f32),
        vmem((1, group_width), f32),
        vmem((top, block_tokens), jnp.int32),
        vmem((top, block_tokens), f32),
        vmem((n_tp, width, part_units), bf16),
        vmem((n_tp, width, part_units), bf16),
        vmem((n_tp, part_units, width), bf16),
        vmem((tokens, width), bf16),
        vmem((n_ep, capacity, tokens), bf16),
        vmem((tokens, slots), bf16),
        vmem((tokens, slots), bf16),
        vmem((n_ep, capacity, width), bf16),
        vmem((n_ep, capacity, width), bf16),
        vmem((n_tp, slots, part_units), f32),
        vmem((n_tp, slots, part_units), f32),
        vmem((slots, units), bf16),
        vmem((D_CHUNKS, n_ep, capacity, d_size), bf16),
        vmem((D_CHUNKS, n_ep, capacity, d_size), bf16),
        vmem((n_tp, tokens, group_width), bf16),
        vmem((WMAX + n_tp * tokens, group_width), bf16),
        vmem((group_width, group_width), bf16),
        vmem((n_tp, tokens, group_width), bf16),
        vmem((D_CHUNKS, tokens, d_size), bf16),
        dma((8,)),
        dma((n_tp, K_CHUNKS)),
        dma((n_tp, K_CHUNKS)),
        dma((n_tp, K_CHUNKS)),
        dma((n_tp, K_CHUNKS)),
        dma((n_tp, D_CHUNKS)),
        dma((n_tp, D_CHUNKS)),
        dma((n_ep,)),
        dma((n_ep,)),
        dma((D_CHUNKS, n_ep)),
        dma((D_CHUNKS, n_ep)),
        dma((n_tp,)),
        dma((n_tp,)),
        dma(()),
        dma(()),
        dma((n_tp,)),
        dma((D_CHUNKS,)),
    ]
    flops = 6 * slots * width * units + 2 * n_tp * tokens * group_width * group_width
    return pl.pallas_call(
        functools.partial(kernel, n_ep, n_tp),
        out_shape=(
            jax.ShapeDtypeStruct((n_tp * tokens, group_width), bf16),
            jax.ShapeDtypeStruct((tokens, width), bf16),
        ),
        in_specs=[anywhere] * 11,
        out_specs=(anywhere, anywhere),
        scratch_shapes=scratch,
        compiler_params=pltpu.CompilerParams(
            collective_id=0, has_side_effects=True, vmem_limit_bytes=67043328
        ),
        cost_estimate=pl.CostEstimate(flops=flops, bytes_accessed=1 << 26, transcendentals=0),
    )(
        mixer_in,
        mixer_gain.reshape(1, width),
        group_weight,
        group_scale,
        expert_in,
        expert_gain.reshape(1, width),
        routes.T,
        route_weight.T,
        gate_weight,
        up_weight,
        down_weight,
    )


def solution(mesh):
    in_specs = (
        P(("ep", "tp"), None),
        P(),
        P("tp", None, None),
        P("tp", None),
        P(("ep", "tp"), None),
        P(),
        P("ep", None),
        P("ep", None),
        P("ep", None, "tp"),
        P("ep", None, "tp"),
        P("ep", "tp", None),
    )
    out_specs = (P("ep", "tp"), P(("ep", "tp"), None))
    return jax.shard_map(shards, mesh=mesh, in_specs=in_specs, out_specs=out_specs, check_vma=False)
```

time: 289 us -> 186 us (0.64); the launches traced: 284 us -> 185 us
  Pallas kernels: 0 us -> 181 us
  blocking collectives: 105 us -> 0 us
  waiting for transfers between devices: 57.2 us -> 0 us
  matrix products: 50.2 us -> 0 us
  starting transfers between devices: 32.4 us -> 0 us
  between operations: 14.1 us -> 0.65 us
  local copies, waits for them, and re-layouts: 15.4 us -> 3.32 us
  other arithmetic: 9.82 us -> 0 us
    pallas_call x0 -> x1, Pallas kernels: none -> 181 us  [shards(): pl.pallas_call(functools.partial(kernel, n_ep, n_tp), out_shape=(jax.Shap...]
    all_to_all x5 -> x0, blocking collectives: 105 us -> none  [the longest x3 83.7 us: shards(): lax.all_to_all(outgoing, 'ep', split_axis=0, concat_axis=0, tiled=True)]
    all_to_all x5 -> x0, waiting for transfers between devices: 51.9 us -> none  [the longest x3 26 us: shards(): lax.all_to_all(result, 'ep', split_axis=0, concat_axis=0, tiled=True)]
    dot_general x20 -> x0, matrix products: 50.2 us -> none  [the longest x3 13.6 us: shards(): jnp.dot(hidden, down_full, preferred_element_type=jnp.float32)]
    all_to_all x5 -> x0, starting transfers between devices: 28.7 us -> none  [the longest x3 21 us: shards(): lax.all_to_all(result, 'ep', split_axis=0, concat_axis=0, tiled=True)]
    unnamed x37 -> x4, local copies, waits for them, and re-layouts: 7.92 us -> 3.32 us
    convert_element_type x3 -> x0, other arithmetic: 4.4 us -> none  [the longest x1 2.9 us: mixer(): total = jnp.concatenate([before, shard_rows], axis=0).astype(jnp.float32)]
    ppermute x1 -> x0, starting transfers between devices: 3.46 us -> none  [from_behind(): return lax.ppermute(x, axis, pairs)]
  transfers between devices with their start and end apart: 10 -> 0, of which waited for: 7 -> 0; matrix products, arithmetic and copies ran while one was open for 23% -> 0% of each run, Pallas kernels for 0% -> 0%
where the time goes in v1:
time: 186 us; the launch traced here: 185 us
  Pallas kernels  181 us (97%)
  local copies, waits for them, and re-layouts  3.32 us (2%)
    pallas_call x1, Pallas kernels, shards(): pl.pallas_call(functools.partial(kernel, n_ep, n_tp), out_shape=(jax.Shap...  181 us

profile of v1, /device:TPU:16, one launch (start us, length us, event | category | flops | bytes accessed | tf_op | source)
XLA Modules:
  0.0 185.2 jit_solution(18112060097871925831)
XLA Ops:
  0.6 181.2 %shard_map.122 = (bf16[512,1024]{1,0:T(8,128)(2,1)}, bf16[128,4096]{1,0:T(8,128)(2,1)}) custom-call(bf16[128,4096]{1,0:T(8,128)(2,1)} %mixer_in.1, f32[1,4096]{1,0:T(1,128)} %bitcast.4, bf16[1,1024,1024]{2,1,0:T(8,128)(2,1)} %group_weight.1, f32[1,1024]{1,0:T(1,128)} %group_scale.1, bf16[128,4096]{1,0:T(8,128)(2,1)} %expert_in.1, f32[1,4096]{1,0:T(1,128)} %bitcast.5, ...), custom_call_target="tpu_custom_call" | custom-call | flops 10737418240 | bytes 67108864 | tf_op jit(solution)/shard_map/pallas_call | solution.py:542
  181.9 0.0 copy-start
  181.9 2.4 %copy.15 = bf16[512,1024]{1,0:T(8,128)(2,1)} copy(bf16[512,1024]{1,0:T(8,128)(2,1)} %get-tuple-element.4) | data formatting | bytes 2097152
  184.2 0.0 copy-done
  184.2 1.0 copy.16
Async XLA Ops:
  181.9 2.4 %copy-start = (bf16[128,4096]{1,0:T(8,128)(2,1)S(1)}, bf16[128,4096]{1,0:T(8,128)(2,1)}, u32[]{:S(2)}) copy-start(bf16[128,4096]{1,0:T(8,128)(2,1)} %get-tuple-element.5) | copy-start | bytes 3145732

commit v2 on v1

v2 whole, which is shorter than its diff:
```python
import functools
import jax
import jax.numpy as jnp
from jax import lax
from jax.experimental import pallas as pl
from jax.experimental.pallas import tpu as pltpu
from jax.sharding import PartitionSpec as P

WMAX = 16
NORM_ROWS = 16
K_CHUNKS = 8
D_CHUNKS = 8

epsilon = 1e-06
clamp_limit = 7.0
sigmoid_slope = 1.702

MESH = pl.DeviceIdType.MESH


def clamped_unit(gate_part, up_part):
    gate_part = jnp.minimum(gate_part, clamp_limit)
    up_part = jnp.clip(up_part, -clamp_limit, clamp_limit)
    return ((up_part + 1.0) * gate_part * jax.nn.sigmoid(sigmoid_slope * gate_part)).astype(
        jnp.bfloat16
    )


def norm_rows(source, gain, at):
    widened = source[pl.ds(at, NORM_ROWS), :].astype(jnp.float32)
    mean = jnp.sum(widened * widened, axis=-1, keepdims=True) * (1.0 / widened.shape[-1])
    return (widened * lax.rsqrt(mean + epsilon) * gain[...]).astype(jnp.bfloat16)


def aligned(value, size):
    return pl.multiple_of(value * size, size)


def kernel(
    n_ep,
    n_tp,
    mixer_in,
    mixer_gain,
    group_weight,
    group_scale,
    expert_in,
    expert_gain,
    routes,
    route_weight,
    gate_w,
    up_w,
    down_w,
    mixed_out,
    expert_out,
    x_in,
    m_in,
    e_gain,
    m_gain,
    scale,
    named,
    shares,
    gate_up,
    down_b,
    normed,
    pick,
    share_high,
    share_low,
    outgoing,
    arrived,
    acc,
    hidden_out,
    hidden,
    result,
    returned,
    m_normed,
    m_rows,
    m_tail,
    g_weight,
    m_out,
    e_out,
    load_sem,
    down_send,
    down_recv,
    out_send,
    out_recv,
    row_send,
    row_recv,
    hid_send,
    hid_recv,
    ret_send,
    ret_recv,
    mix_send,
    mix_recv,
    tail_send,
    tail_recv,
    halo_send,
    halo_recv,
    m_store,
    e_store,
):
    ep = lax.axis_index("ep")
    tp = lax.axis_index("tp")
    tokens, width = x_in.shape
    group_width = g_weight.shape[0]
    n_groups, group, sub, units = hidden.shape
    rounds = n_groups // 2
    slots = n_ep * rounds * sub
    part_units = units // n_tp
    k_size = width // K_CHUNKS
    d_size = width // D_CHUNKS

    def peer(i):
        return jnp.bitwise_xor(ep, i)

    loads = [
        pltpu.make_async_copy(origin, target, load_sem.at[i])
        for i, (origin, target) in enumerate(
            [
                (expert_in, x_in),
                (expert_gain, e_gain),
                (routes, named),
                (route_weight, shares),
                (gate_w.at[0], gate_up.at[:, 0:part_units]),
                (up_w.at[0], gate_up.at[:, part_units : 2 * part_units]),
                (mixer_in, m_in),
                (mixer_gain, m_gain),
                (group_scale, scale),
                (group_weight.at[0], g_weight),
            ]
        )
    ]
    for load in loads:
        load.start()

    barrier = pltpu.get_barrier_semaphore()
    for r in range(1, n_tp):
        pl.semaphore_signal(barrier, inc=1, device_id={"tp": tp ^ r}, device_id_type=MESH)

    @pl.loop(1, n_ep)
    def _(i):
        pl.semaphore_signal(barrier, inc=1, device_id={"ep": peer(i)}, device_id_type=MESH)

    bits = []
    while (1 << len(bits)) < n_tp:
        bits.insert(0, 1 << len(bits))
    forwards = {r: [r | b for b in bits if r == 0 or b < (r & -r)] for r in range(n_tp)}
    order = [0] + sorted(range(1, n_tp), key=lambda r: (r & (n_tp // 2) > 0, bin(r).count("1")))
    relays = [r for r in order[1:] if forwards[r]]
    leaves = [r for r in order[1:] if not forwards[r]]

    def down_copy(r, j):
        low = r & -r
        span = (slice(None), pl.ds(aligned(j, d_size), d_size))
        origin = down_w.at[(0,) + span] if r == low else down_b.at[(r ^ low,) + span]
        if r == 0:
            return pltpu.make_async_copy(origin, down_b.at[(0,) + span], down_recv.at[0, j])
        return pltpu.make_async_remote_copy(
            src_ref=origin,
            dst_ref=down_b.at[(r,) + span],
            send_sem=down_send.at[r, j],
            recv_sem=down_recv.at[r, j],
            device_id={"tp": tp ^ low},
            device_id_type=MESH,
        )

    def row_copy(r, u, i):
        low = r & -r
        return pltpu.make_async_remote_copy(
            src_ref=arrived.at[u, i, r ^ low],
            dst_ref=arrived.at[u, i, r],
            send_sem=row_send.at[r, u, i],
            recv_sem=row_recv.at[r, u, i],
            device_id={"tp": tp ^ low},
            device_id_type=MESH,
        )

    def start_down(first, last):
        @pl.loop(first, last)
        def _(j):
            for r in forwards[0]:
                down_copy(r, j).start()

    @pl.loop(0, D_CHUNKS)
    def _(j):
        down_copy(0, j).start()

    pl.semaphore_wait(barrier, n_ep - 1 + n_tp - 1)
    start_down(0, 1)

    for load in loads[:4]:
        load.wait()
    mine = pl.ds(aligned(tp, tokens), tokens)
    own = named[:, mine]
    own_share = shares[:, mine]
    top = own.shape[0]
    experts = lax.broadcasted_iota(jnp.int32, (n_ep, tokens), 0)
    onehot = [
        (experts == jnp.broadcast_to(own[k : k + 1, :], (n_ep, tokens))).astype(jnp.float32)
        for k in range(top)
    ]
    per_token = functools.reduce(lambda a, b: a + b, onehot)
    before = (
        lax.broadcasted_iota(jnp.int32, (tokens, tokens), 0)
        < lax.broadcasted_iota(jnp.int32, (tokens, tokens), 1)
    ).astype(jnp.bfloat16)
    earlier = jnp.dot(per_token.astype(jnp.bfloat16), before, preferred_element_type=jnp.float32)
    slot_rows = lax.broadcasted_iota(jnp.int32, (slots, tokens), 0)
    picked = jnp.zeros((slots, tokens), jnp.float32)
    spread = jnp.zeros((slots, tokens), jnp.float32)
    shift = sub.bit_length() - 1
    for k in range(top):
        rank = jnp.sum(onehot[k] * earlier, axis=0, keepdims=True).astype(jnp.int32)
        away = jnp.bitwise_xor(own[k : k + 1, :], ep)
        turn = lax.shift_right_logical(rank, jnp.full_like(rank, shift))
        far = jnp.where(away >= group, 1, 0)
        slot = ((far * rounds + turn) * group + away - far * group) * sub + rank - turn * sub
        match = slot_rows == jnp.broadcast_to(slot, (slots, tokens))
        picked = picked + jnp.where(match, 1.0, 0.0)
        spread = spread + jnp.where(
            match, jnp.broadcast_to(own_share[k : k + 1, :], (slots, tokens)), 0.0
        )
    picked = picked.reshape(2, rounds, group * sub, tokens).astype(jnp.bfloat16)
    for half in range(2):
        pick[:, half * group * sub : (half + 1) * group * sub, :] = picked[half]
    spread = spread.T
    high = spread.astype(jnp.bfloat16)
    share_high[...] = high
    share_low[...] = (spread - high.astype(jnp.float32)).astype(jnp.bfloat16)

    @pl.loop(0, tokens // NORM_ROWS)
    def _(i):
        at = aligned(i, NORM_ROWS)
        normed[pl.ds(at, NORM_ROWS), :] = norm_rows(x_in, e_gain, at)

    def send_rows(u, i):
        half = u // rounds
        return pltpu.make_async_remote_copy(
            src_ref=outgoing.at[u, i],
            dst_ref=arrived.at[u, i, 0],
            send_sem=out_send.at[u, i],
            recv_sem=out_recv.at[u, i],
            device_id={"ep": peer(half * group + i)},
            device_id_type=MESH,
        )

    sequence = [0, rounds] + list(range(1, rounds)) + list(range(rounds + 1, n_groups))

    def send_group(u):
        @pl.loop(0 if u >= rounds else 1, group)
        def _(i):
            send_rows(u, i).start()

    for k in range(rounds):
        rows = jnp.dot(pick[k], normed[...], preferred_element_type=jnp.float32)
        rows = rows.astype(jnp.bfloat16).reshape(2, group, sub, width)
        arrived[k, 0, 0] = rows[0, 0]
        for half in range(2):
            outgoing[half * rounds + k] = rows[half]
        for r in forwards[0]:
            row_copy(r, k, 0).start()
        for u in (0, rounds) if k == 0 else (k,):
            send_group(u)
    for u in range(rounds + 1, n_groups):
        send_group(u)

    for load in loads[4:]:
        load.wait()

    @pl.loop(0, tokens // NORM_ROWS)
    def _(i):
        at = aligned(i, NORM_ROWS)
        rows = norm_rows(m_in, m_gain, at)
        for g in range(n_tp):
            m_normed[g, pl.ds(at, NORM_ROWS), :] = rows[:, g * group_width : (g + 1) * group_width]

    own_rows = pl.ds(pl.multiple_of(WMAX + tp * tokens, WMAX), tokens)
    m_rows[own_rows, :] = m_normed[tp]

    last = n_tp - 1

    def tail_copy(r):
        return pltpu.make_async_remote_copy(
            src_ref=m_normed.at[last ^ r, tokens - WMAX : tokens, :],
            dst_ref=m_tail,
            send_sem=tail_send.at[r],
            recv_sem=tail_recv,
            device_id={"tp": tp ^ r},
            device_id_type=MESH,
        )

    halo = pltpu.make_async_remote_copy(
        src_ref=m_tail,
        dst_ref=m_rows.at[0:WMAX, :],
        send_sem=halo_send,
        recv_sem=halo_recv,
        device_id={"ep": lax.rem(ep + 1, n_ep)},
        device_id_type=MESH,
    )

    @pl.when(tp == last)
    def _():
        for r in range(1, n_tp):
            tail_copy(r).start()
        m_tail[...] = m_normed[last, tokens - WMAX : tokens, :]


    def send_mix(r):
        return pltpu.make_async_remote_copy(
            src_ref=m_normed.at[tp ^ r],
            dst_ref=m_rows.at[own_rows, :],
            send_sem=mix_send.at[r],
            recv_sem=mix_recv.at[r],
            device_id={"tp": tp ^ r},
            device_id_type=MESH,
        )

    def take(u):
        @pl.loop(0 if u >= rounds else 1, group)
        def _(i):
            send_rows(u, i).wait_recv()
            for r in forwards[0]:
                row_copy(r, u, i).start()

    def relay(u):
        for r in relays:

            @pl.loop(0, group)
            def _(i):
                row_copy(r, u, i).wait_recv()
                for target in forwards[r]:
                    row_copy(target, u, i).start()

    def hid_copy(r, u):
        return pltpu.make_async_remote_copy(
            src_ref=hidden_out.at[u, r],
            dst_ref=hidden.at[u, :, :, r * part_units : (r + 1) * part_units],
            send_sem=hid_send.at[r, u],
            recv_sem=hid_recv.at[r, u],
            device_id={"tp": tp ^ r},
            device_id_type=MESH,
        )

    def work(u):
        for r in leaves:

            @pl.loop(0, group)
            def _(i):
                row_copy(r, u, i).wait_recv()

        @pl.loop(0, K_CHUNKS)
        def _(k):
            span = pl.ds(aligned(k, k_size), k_size)
            rows = arrived[u, :, :, :, span].reshape(group * n_tp * sub, k_size)
            product = jnp.dot(rows, gate_up[span, :], preferred_element_type=jnp.float32)

            @pl.when(k == 0)
            def _():
                acc[...] = product

            @pl.when(k > 0)
            def _():
                acc[...] += product

        units_of = clamped_unit(acc[:, :part_units], acc[:, part_units:])
        units_of = units_of.reshape(group, n_tp, sub, part_units)
        hidden[u, :, :, 0:part_units] = units_of[:, 0]
        for r in range(1, n_tp):
            hidden_out[u, r] = units_of[:, r]
            hid_copy(r, u).start()

    for step in range(len(sequence) + 2):
        if step < len(sequence):
            take(sequence[step])
        if step == min(1, len(sequence) - 1):

            @pl.when(tp != last)
            def _():
                tail_copy(1).wait_recv()

            halo.start()
        if step == len(sequence) and step >= 2:
            work(sequence[step - 2])
        if 1 <= step <= len(sequence):
            relay(sequence[step - 1])
        if step >= 2 and step != len(sequence) or step == len(sequence) + 1:
            work(sequence[step - 2])

    start_down(1, D_CHUNKS)
    for r in range(1, n_tp):
        send_mix(r).start()

    for u in sequence:
        for r in range(1, n_tp):
            hid_copy(r, u).wait_recv()

    def send_back(j, half, i):
        block = (j, slice(half * rounds, (half + 1) * rounds), i)
        return pltpu.make_async_remote_copy(
            src_ref=result.at[block],
            dst_ref=returned.at[block],
            send_sem=ret_send.at[j, half, i],
            recv_sem=ret_recv.at[j, half, i],
            device_id={"ep": peer(half * group + i)},
            device_id_type=MESH,
        )

    def down_arrive(j):
        down_copy(0, j).wait()
        for r in relays:
            down_copy(r, j).wait_recv()
            for target in forwards[r]:
                down_copy(target, j).start()
        for r in leaves:
            down_copy(r, j).wait_recv()

    @pl.loop(0, D_CHUNKS)
    def _(j):
        down_arrive(j)
        weight = down_b[:, :, pl.ds(aligned(j, d_size), d_size)].reshape(units, d_size)
        rows = hidden[...].reshape(slots, units)
        product = jnp.dot(rows, weight, preferred_element_type=jnp.float32)
        result[j] = product.astype(jnp.bfloat16).reshape(n_groups, group, sub, d_size)

        for half in (1, 0):

            @pl.loop(1 - half, group)
            def _(i):
                send_back(j, half, i).start()

        returned[j, 0:rounds, 0] = result[j, 0:rounds, 0]

    for r in range(1, n_tp):
        theirs = pl.ds(pl.multiple_of(WMAX + (tp ^ r) * tokens, WMAX), tokens)
        pltpu.make_async_remote_copy(
            src_ref=m_normed.at[tp ^ r],
            dst_ref=m_rows.at[theirs, :],
            send_sem=mix_send.at[r],
            recv_sem=mix_recv.at[r],
            device_id={"tp": tp ^ r},
            device_id_type=MESH,
        ).wait_recv()
    halo.wait_recv()
    window = 2 << tp
    span_rows = tokens + WMAX
    here = lax.broadcasted_iota(jnp.int32, (tokens, span_rows), 0)
    there = lax.broadcasted_iota(jnp.int32, (tokens, span_rows), 1)
    back = here + WMAX - there
    inside = (back >= 0) & (back < window)
    row = lax.broadcasted_iota(jnp.int32, (tokens, 1), 0)
    stores = []
    for b in range(n_tp):
        position = (ep * n_tp + b) * tokens
        band = (inside & (there + position >= WMAX)).astype(jnp.bfloat16)
        values = m_rows[b * tokens : b * tokens + span_rows, :]
        total = jnp.dot(band, values, preferred_element_type=jnp.float32)
        counts = jnp.minimum(row + position + 1, window).astype(jnp.float32)
        pooled = (total / counts - values[WMAX:, :].astype(jnp.float32)).astype(jnp.bfloat16)
        product = jnp.dot(pooled, g_weight[...], preferred_element_type=jnp.float32)
        m_out[b] = (product * scale[...]).astype(jnp.bfloat16)
        store = pltpu.make_async_copy(
            m_out.at[b], mixed_out.at[b * tokens : (b + 1) * tokens, :], m_store.at[b]
        )
        store.start()
        stores.append(store)

    def write_out(j):
        return pltpu.make_async_copy(
            e_out.at[j], expert_out.at[:, pl.ds(aligned(j, d_size), d_size)], e_store.at[j]
        )

    @pl.loop(0, D_CHUNKS)
    def _(j):
        for half in range(2):

            @pl.loop(1 - half, group)
            def _(i):
                send_back(j, half, i).wait_recv()

        rows = returned[j].reshape(slots, d_size)
        e_out[j] = (
            jnp.dot(share_high[...], rows, preferred_element_type=jnp.float32)
            + jnp.dot(share_low[...], rows, preferred_element_type=jnp.float32)
        ).astype(jnp.bfloat16)
        write_out(j).start()

    for r in range(1, n_tp):

        @pl.loop(0, D_CHUNKS)
        def _(j):
            down_copy(r, j).wait_send()

        @pl.loop(0, n_groups)
        def _(u):
            hid_copy(r, u).wait_send()

        @pl.loop(0, n_groups)
        def _(u):
            @pl.loop(0, group)
            def _(i):
                row_copy(r, u, i).wait_send()

        send_mix(r).wait_send()
    halo.wait_send()

    @pl.when(tp == last)
    def _():
        for r in range(1, n_tp):
            tail_copy(r).wait_send()

    for half in range(2):

        @pl.loop(1 - half, group)
        def _(i):
            for u in range(half * rounds, (half + 1) * rounds):
                send_rows(u, i).wait_send()

            @pl.loop(0, D_CHUNKS)
            def _(j):
                send_back(j, half, i).wait_send()

    @pl.loop(0, D_CHUNKS)
    def _(j):
        write_out(j).wait()

    for store in stores:
        store.wait()


def shards(
    mixer_in,
    mixer_gain,
    group_weight,
    group_scale,
    expert_in,
    expert_gain,
    routes,
    route_weight,
    gate_weight,
    up_weight,
    down_weight,
):
    n_ep = lax.axis_size("ep")
    n_tp = lax.axis_size("tp")
    tokens, width = expert_in.shape
    group_width = group_weight.shape[-1]
    block_tokens, top = routes.shape
    part_units = gate_weight.shape[-1]
    units = part_units * n_tp
    capacity = max(2, 3 * tokens * top // (2 * n_ep))
    capacity = -(-capacity // 8) * 8
    slots = n_ep * capacity
    sub = 16 if capacity % 16 == 0 else 8
    rounds = capacity // sub
    groups = 2 * rounds
    group = n_ep // 2
    d_size = width // D_CHUNKS
    bf16, f32 = jnp.bfloat16, jnp.float32
    vmem = pltpu.VMEM
    dma = pltpu.SemaphoreType.DMA
    anywhere = pl.BlockSpec(memory_space=pl.ANY)
    scratch = [
        vmem((tokens, width), bf16),
        vmem((tokens, width), bf16),
        vmem((1, width), f32),
        vmem((1, width), f32),
        vmem((1, group_width), f32),
        vmem((top, block_tokens), jnp.int32),
        vmem((top, block_tokens), f32),
        vmem((width, 2 * part_units), bf16),
        vmem((n_tp, part_units, width), bf16),
        vmem((tokens, width), bf16),
        vmem((rounds, n_ep * sub, tokens), bf16),
        vmem((tokens, slots), bf16),
        vmem((tokens, slots), bf16),
        vmem((groups, group, sub, width), bf16),
        vmem((groups, group, n_tp, sub, width), bf16),
        vmem((group * n_tp * sub, 2 * part_units), f32),
        vmem((groups, n_tp, group, sub, part_units), bf16),
        vmem((groups, group, sub, units), bf16),
        vmem((D_CHUNKS, groups, group, sub, d_size), bf16),
        vmem((D_CHUNKS, groups, group, sub, d_size), bf16),
        vmem((n_tp, tokens, group_width), bf16),
        vmem((WMAX + n_tp * tokens, group_width), bf16),
        vmem((WMAX, group_width), bf16),
        vmem((group_width, group_width), bf16),
        vmem((n_tp, tokens, group_width), bf16),
        vmem((D_CHUNKS, tokens, d_size), bf16),
        dma((10,)),
        dma((n_tp, D_CHUNKS)),
        dma((n_tp, D_CHUNKS)),
        dma((groups, group)),
        dma((groups, group)),
        dma((n_tp, groups, group)),
        dma((n_tp, groups, group)),
        dma((n_tp, groups)),
        dma((n_tp, groups)),
        dma((D_CHUNKS, 2, group)),
        dma((D_CHUNKS, 2, group)),
        dma((n_tp,)),
        dma((n_tp,)),
        dma((n_tp,)),
        dma(()),
        dma(()),
        dma(()),
        dma((n_tp,)),
        dma((D_CHUNKS,)),
    ]
    flops = 6 * slots * width * units + 2 * n_tp * tokens * group_width * group_width
    return pl.pallas_call(
        functools.partial(kernel, n_ep, n_tp),
        out_shape=(
            jax.ShapeDtypeStruct((n_tp * tokens, group_width), bf16),
            jax.ShapeDtypeStruct((tokens, width), bf16),
        ),
        in_specs=[anywhere] * 11,
        out_specs=(anywhere, anywhere),
        scratch_shapes=scratch,
        compiler_params=pltpu.CompilerParams(
            collective_id=0, has_side_effects=True, vmem_limit_bytes=67043328
        ),
        cost_estimate=pl.CostEstimate(flops=flops, bytes_accessed=1 << 26, transcendentals=0),
    )(
        mixer_in,
        mixer_gain.reshape(1, width),
        group_weight,
        group_scale,
        expert_in,
        expert_gain.reshape(1, width),
        routes.T,
        route_weight.T,
        gate_weight,
        up_weight,
        down_weight,
    )


def solution(mesh):
    in_specs = (
        P(("ep", "tp"), None),
        P(),
        P("tp", None, None),
        P("tp", None),
        P(("ep", "tp"), None),
        P(),
        P("ep", None),
        P("ep", None),
        P("ep", None, "tp"),
        P("ep", None, "tp"),
        P("ep", "tp", None),
    )
    out_specs = (P("ep", "tp"), P(("ep", "tp"), None))
    return jax.shard_map(shards, mesh=mesh, in_specs=in_specs, out_specs=out_specs, check_vma=False)
```

time: 186 us -> 174 us (0.935)
  Pallas kernels: 181 us -> 168 us
    pallas_call x1, Pallas kernels: 181 us -> 168 us  [shards(): pl.pallas_call(functools.partial(kernel, n_ep, n_tp), out_shape=(jax.Shap...]
where the time goes in v2:
time: 174 us; the launch traced here: 172 us
  Pallas kernels  168 us (97%)
  local copies, waits for them, and re-layouts  3.32 us (2%)
    pallas_call x1, Pallas kernels, shards(): pl.pallas_call(functools.partial(kernel, n_ep, n_tp), out_shape=(jax.Shap...  168 us

profile of v2, /device:TPU:16, one launch (start us, length us, event | category | flops | bytes accessed | tf_op | source)
XLA Modules:
  0.0 172.4 jit_solution(582455443693139404)
XLA Ops:
  0.6 168.5 %shard_map.122 = (bf16[512,1024]{1,0:T(8,128)(2,1)}, bf16[128,4096]{1,0:T(8,128)(2,1)}) custom-call(bf16[128,4096]{1,0:T(8,128)(2,1)} %mixer_in.1, f32[1,4096]{1,0:T(1,128)} %bitcast.4, bf16[1,1024,1024]{2,1,0:T(8,128)(2,1)} %group_weight.1, f32[1,1024]{1,0:T(1,128)} %group_scale.1, bf16[128,4096]{1,0:T(8,128)(2,1)} %expert_in.1, f32[1,4096]{1,0:T(1,128)} %bitcast.5, ...), custom_call_target="tpu_custom_call" | custom-call | flops 10737418240 | bytes 67108864 | tf_op jit(solution)/shard_map/pallas_call | solution.py:609
  169.1 0.0 copy-start
  169.1 2.4 %copy.15 = bf16[512,1024]{1,0:T(8,128)(2,1)} copy(bf16[512,1024]{1,0:T(8,128)(2,1)} %get-tuple-element.4) | data formatting | bytes 2097152
  171.5 0.0 copy-done
  171.5 1.0 copy.16
Async XLA Ops:
  169.1 2.4 %copy-start = (bf16[128,4096]{1,0:T(8,128)(2,1)S(1)}, bf16[128,4096]{1,0:T(8,128)(2,1)}, u32[]{:S(2)}) copy-start(bf16[128,4096]{1,0:T(8,128)(2,1)} %get-tuple-element.5) | copy-start | bytes 3145732

commit v3 on v2

--- a/solution.py
+++ b/solution.py
@@ -10,6 +10,8 @@
 NORM_ROWS = 16
 K_CHUNKS = 8
 D_CHUNKS = 8
+FIRST = 1
+SECOND = 2
 
 epsilon = 1e-06
 clamp_limit = 7.0
@@ -63,8 +65,9 @@
     down_b,
     normed,
     pick,
-    share_high,
-    share_low,
+    share_near,
+    share_far,
+    share_in,
     outgoing,
     arrived,
     acc,
@@ -72,6 +75,9 @@
     hidden,
     result,
     returned,
+    gathered,
+    partial_out,
+    partial_in,
     m_normed,
     m_rows,
     m_tail,
@@ -89,6 +95,12 @@
     hid_recv,
     ret_send,
     ret_recv,
+    share_send,
+    share_recv,
+    col_send,
+    col_recv,
+    part_send,
+    part_recv,
     mix_send,
     mix_recv,
     tail_send,
@@ -105,12 +117,17 @@
     n_groups, group, sub, units = hidden.shape
     rounds = n_groups // 2
     slots = n_ep * rounds * sub
+    quarter = n_ep // 4
+    lag = 1
+    near_lag = 2
     part_units = units // n_tp
     k_size = width // K_CHUNKS
     d_size = width // D_CHUNKS
 
     def peer(i):
         return jnp.bitwise_xor(ep, i)
+
+    inner = jnp.bitwise_xor(lax.rem(lax.div(ep, quarter), 2), lax.div(ep, group))
 
     loads = [
         pltpu.make_async_copy(origin, target, load_sem.at[i])
@@ -185,7 +202,7 @@
         down_copy(0, j).start()
 
     pl.semaphore_wait(barrier, n_ep - 1 + n_tp - 1)
-    start_down(0, 1)
+    start_down(0, FIRST)
 
     for load in loads[:4]:
         load.wait()
@@ -224,8 +241,18 @@
         pick[:, half * group * sub : (half + 1) * group * sub, :] = picked[half]
     spread = spread.T
     high = spread.astype(jnp.bfloat16)
-    share_high[...] = high
-    share_low[...] = (spread - high.astype(jnp.float32)).astype(jnp.bfloat16)
+    low = (spread - high.astype(jnp.float32)).astype(jnp.bfloat16)
+    for i, part in enumerate((high, low)):
+        share_near[i] = part[:, : slots // 2]
+        share_far[i] = part[:, slots // 2 :]
+    share_copy = pltpu.make_async_remote_copy(
+        src_ref=share_far,
+        dst_ref=share_in.at[1 - inner],
+        send_sem=share_send,
+        recv_sem=share_recv.at[1 - inner],
+        device_id={"ep": peer(group + quarter * inner)},
+        device_id_type=MESH,
+    )
 
     @pl.loop(0, tokens // NORM_ROWS)
     def _(i):
@@ -262,6 +289,7 @@
             send_group(u)
     for u in range(rounds + 1, n_groups):
         send_group(u)
+    share_copy.start()
 
     for load in loads[4:]:
         load.wait()
@@ -380,12 +408,13 @@
             halo.start()
         if step == len(sequence) and step >= 2:
             work(sequence[step - 2])
+            start_down(FIRST, SECOND)
         if 1 <= step <= len(sequence):
             relay(sequence[step - 1])
         if step >= 2 and step != len(sequence) or step == len(sequence) + 1:
             work(sequence[step - 2])
 
-    start_down(1, D_CHUNKS)
+    start_down(SECOND, D_CHUNKS)
     for r in range(1, n_tp):
         send_mix(r).start()
 
@@ -393,16 +422,73 @@
         for r in range(1, n_tp):
             hid_copy(r, u).wait_recv()
 
-    def send_back(j, half, i):
-        block = (j, slice(half * rounds, (half + 1) * rounds), i)
-        return pltpu.make_async_remote_copy(
-            src_ref=result.at[block],
-            dst_ref=returned.at[block],
-            send_sem=ret_send.at[j, half, i],
-            recv_sem=ret_recv.at[j, half, i],
-            device_id={"ep": peer(half * group + i)},
-            device_id_type=MESH,
-        )
+    far = slice(rounds, n_groups)
+
+    def send_back(j, i):
+        return pltpu.make_async_remote_copy(
+            src_ref=result.at[j, 0:rounds, i],
+            dst_ref=returned.at[j, :, i],
+            send_sem=ret_send.at[j, i],
+            recv_sem=ret_recv.at[j, i],
+            device_id={"ep": peer(i)},
+            device_id_type=MESH,
+        )
+
+    def send_near(j):
+        @pl.loop(1, group)
+        def _(i):
+            send_back(j, i).start()
+
+    def bit_of(i):
+        return lax.rem(lax.div(i, quarter), 2)
+
+    def collect(j, i, kind, step):
+        return pltpu.make_async_remote_copy(
+            src_ref=result.at[j, far, i],
+            dst_ref=gathered.at[kind, j, :, i],
+            send_sem=col_send.at[j, i],
+            recv_sem=col_recv.at[kind, j, i],
+            device_id={"ep": peer(step)},
+            device_id_type=MESH,
+        )
+
+    def collect_out(j, i):
+        kind = jnp.bitwise_xor(bit_of(i), inner)
+        step = lax.rem(i, quarter) + (1 - inner) * quarter
+        return kind, step
+
+    def collect_in(i, kind):
+        return lax.rem(i, quarter) + (1 - jnp.bitwise_xor(bit_of(i), kind)) * quarter
+
+    def partial_copy(kind, j):
+        return pltpu.make_async_remote_copy(
+            src_ref=partial_out.at[kind, j],
+            dst_ref=partial_in.at[j],
+            send_sem=part_send.at[kind, j],
+            recv_sem=part_recv.at[j],
+            device_id={"ep": peer(group + (1 - kind) * quarter)},
+            device_id_type=MESH,
+        )
+
+    def sum_far(j):
+        @pl.when(inner == 1)
+        def _():
+            for kind in (1, 0):
+
+                @pl.loop(0, group)
+                def _(i):
+                    step = collect_in(i, kind)
+
+                    @pl.when(step > 0)
+                    def _():
+                        collect(j, i, kind, step).wait_recv()
+
+                rows = gathered[kind, j].reshape(slots // 2, d_size)
+                partial_out[kind, j] = (
+                    jnp.dot(share_in[kind, 0], rows, preferred_element_type=jnp.float32)
+                    + jnp.dot(share_in[kind, 1], rows, preferred_element_type=jnp.float32)
+                ).astype(jnp.bfloat16)
+                partial_copy(kind, j).start()
 
     def down_arrive(j):
         down_copy(0, j).wait()
@@ -413,6 +499,18 @@
         for r in leaves:
             down_copy(r, j).wait_recv()
 
+    @pl.when(inner == 1)
+    def _():
+        for kind in range(2):
+            pltpu.make_async_remote_copy(
+                src_ref=share_far,
+                dst_ref=share_in.at[kind],
+                send_sem=share_send,
+                recv_sem=share_recv.at[kind],
+                device_id={"ep": peer(group)},
+                device_id_type=MESH,
+            ).wait_recv()
+
     @pl.loop(0, D_CHUNKS)
     def _(j):
         down_arrive(j)
@@ -421,13 +519,35 @@
         product = jnp.dot(rows, weight, preferred_element_type=jnp.float32)
         result[j] = product.astype(jnp.bfloat16).reshape(n_groups, group, sub, d_size)
 
-        for half in (1, 0):
-
-            @pl.loop(1 - half, group)
-            def _(i):
-                send_back(j, half, i).start()
-
-        returned[j, 0:rounds, 0] = result[j, 0:rounds, 0]
+        @pl.loop(0, group)
+        def _(i):
+            kind, step = collect_out(j, i)
+
+            @pl.when(step > 0)
+            def _():
+                collect(j, i, kind, step).start()
+
+            @pl.when(step == 0)
+            def _():
+                gathered[kind, j, :, i] = result[j, far, i]
+
+        returned[j, :, 0] = result[j, 0:rounds, 0]
+
+        @pl.when(j >= near_lag)
+        def _():
+            send_near(j - near_lag)
+
+        @pl.when(j >= lag)
+        def _():
+            sum_far(j - lag)
+
+    @pl.loop(D_CHUNKS - near_lag, D_CHUNKS)
+    def _(j):
+        send_near(j)
+
+    @pl.loop(D_CHUNKS - lag, D_CHUNKS)
+    def _(j):
+        sum_far(j)
 
     for r in range(1, n_tp):
         theirs = pl.ds(pl.multiple_of(WMAX + (tp ^ r) * tokens, WMAX), tokens)
@@ -470,16 +590,16 @@
 
     @pl.loop(0, D_CHUNKS)
     def _(j):
-        for half in range(2):
-
-            @pl.loop(1 - half, group)
-            def _(i):
-                send_back(j, half, i).wait_recv()
-
-        rows = returned[j].reshape(slots, d_size)
+        @pl.loop(1, group)
+        def _(i):
+            send_back(j, i).wait_recv()
+
+        partial_copy(0, j).wait_recv()
+        rows = returned[j].reshape(slots // 2, d_size)
         e_out[j] = (
-            jnp.dot(share_high[...], rows, preferred_element_type=jnp.float32)
-            + jnp.dot(share_low[...], rows, preferred_element_type=jnp.float32)
+            jnp.dot(share_near[0], rows, preferred_element_type=jnp.float32)
+            + jnp.dot(share_near[1], rows, preferred_element_type=jnp.float32)
+            + partial_in[j].astype(jnp.float32)
         ).astype(jnp.bfloat16)
         write_out(j).start()
 
@@ -507,6 +627,8 @@
         for r in range(1, n_tp):
             tail_copy(r).wait_send()
 
+    share_copy.wait_send()
+
     for half in range(2):
 
         @pl.loop(1 - half, group)
@@ -514,9 +636,24 @@
             for u in range(half * rounds, (half + 1) * rounds):
                 send_rows(u, i).wait_send()
 
-            @pl.loop(0, D_CHUNKS)
-            def _(j):
-                send_back(j, half, i).wait_send()
+    @pl.loop(0, D_CHUNKS)
+    def _(j):
+        @pl.loop(0, group)
+        def _(i):
+            kind, step = collect_out(j, i)
+
+            @pl.when(step > 0)
+            def _():
+                collect(j, i, kind, step).wait_send()
+
+        @pl.loop(1, group)
+        def _(i):
+            send_back(j, i).wait_send()
+
+        @pl.when(inner == 1)
+        def _():
+            for kind in range(2):
+                partial_copy(kind, j).wait_send()
 
     @pl.loop(0, D_CHUNKS)
     def _(j):
@@ -570,15 +707,19 @@
         vmem((n_tp, part_units, width), bf16),
         vmem((tokens, width), bf16),
         vmem((rounds, n_ep * sub, tokens), bf16),
-        vmem((tokens, slots), bf16),
-        vmem((tokens, slots), bf16),
+        vmem((2, tokens, slots // 2), bf16),
+        vmem((2, tokens, slots // 2), bf16),
+        vmem((2, 2, tokens, slots // 2), bf16),
         vmem((groups, group, sub, width), bf16),
         vmem((groups, group, n_tp, sub, width), bf16),
         vmem((group * n_tp * sub, 2 * part_units), f32),
         vmem((groups, n_tp, group, sub, part_units), bf16),
         vmem((groups, group, sub, units), bf16),
         vmem((D_CHUNKS, groups, group, sub, d_size), bf16),
-        vmem((D_CHUNKS, groups, group, sub, d_size), bf16),
+        vmem((D_CHUNKS, rounds, group, sub, d_size), bf16),
+        vmem((2, D_CHUNKS, rounds, group, sub, d_size), bf16),
+        vmem((2, D_CHUNKS, tokens, d_size), bf16),
+        vmem((D_CHUNKS, tokens, d_size), bf16),
         vmem((n_tp, tokens, group_width), bf16),
         vmem((WMAX + n_tp * tokens, group_width), bf16),
         vmem((WMAX, group_width), bf16),
@@ -594,8 +735,14 @@
         dma((n_tp, groups, group)),
         dma((n_tp, groups)),
         dma((n_tp, groups)),
-        dma((D_CHUNKS, 2, group)),
-        dma((D_CHUNKS, 2, group)),
+        dma((D_CHUNKS, group)),
+        dma((D_CHUNKS, group)),
+        dma(()),
+        dma((2,)),
+        dma((D_CHUNKS, group)),
+        dma((2, D_CHUNKS, group)),
+        dma((2, D_CHUNKS)),
+        dma((D_CHUNKS,)),
         dma((n_tp,)),
         dma((n_tp,)),
         dma((n_tp,)),

time: 174 us -> 161 us (0.925); the launches traced: 172 us -> 161 us
  Pallas kernels: 168 us -> 157 us
    pallas_call x1, Pallas kernels: 168 us -> 157 us  [shards(): pl.pallas_call(functools.partial(kernel, n_ep, n_tp), out_shape=(jax.Shap...]
where the time goes in v3:
time: 161 us
  Pallas kernels  157 us (98%)
  local copies, waits for them, and re-layouts  3.32 us (2%)
    pallas_call x1, Pallas kernels, shards(): pl.pallas_call(functools.partial(kernel, n_ep, n_tp), out_shape=(jax.Shap...  157 us
    unnamed x4, local copies, waits for them, and re-layouts  3.32 us

profile of v3, /device:TPU:16, one launch (start us, length us, event | category | flops | bytes accessed | tf_op | source)
XLA Modules:
  0.0 161.2 jit_solution(18233902313985004983)
XLA Ops:
  0.6 157.3 %shard_map.122 = (bf16[512,1024]{1,0:T(8,128)(2,1)}, bf16[128,4096]{1,0:T(8,128)(2,1)}) custom-call(bf16[128,4096]{1,0:T(8,128)(2,1)} %mixer_in.1, f32[1,4096]{1,0:T(1,128)} %bitcast.4, bf16[1,1024,1024]{2,1,0:T(8,128)(2,1)} %group_weight.1, f32[1,1024]{1,0:T(1,128)} %group_scale.1, bf16[128,4096]{1,0:T(8,128)(2,1)} %expert_in.1, f32[1,4096]{1,0:T(1,128)} %bitcast.5, ...), custom_call_target="tpu_custom_call" | custom-call | flops 10737418240 | bytes 67108864 | tf_op jit(solution)/shard_map/pallas_call | solution.py:756
  157.9 0.0 copy-start
  157.9 2.4 %copy.15 = bf16[512,1024]{1,0:T(8,128)(2,1)} copy(bf16[512,1024]{1,0:T(8,128)(2,1)} %get-tuple-element.4) | data formatting | bytes 2097152
  160.3 0.0 copy-done
  160.3 1.0 copy.16
Async XLA Ops:
  157.9 2.4 %copy-start = (bf16[128,4096]{1,0:T(8,128)(2,1)S(1)}, bf16[128,4096]{1,0:T(8,128)(2,1)}, u32[]{:S(2)}) copy-start(bf16[128,4096]{1,0:T(8,128)(2,1)} %get-tuple-element.5) | copy-start | bytes 3145732

commit v4 on v3

--- a/solution.py
+++ b/solution.py
@@ -9,7 +9,7 @@
 WMAX = 16
 NORM_ROWS = 16
 K_CHUNKS = 8
-D_CHUNKS = 8
+D_CHUNKS = 16
 FIRST = 1
 SECOND = 2
 
@@ -91,6 +91,7 @@
     out_recv,
     row_send,
     row_recv,
+    leaf_recv,
     hid_send,
     hid_recv,
     ret_send,
@@ -118,8 +119,8 @@
     rounds = n_groups // 2
     slots = n_ep * rounds * sub
     quarter = n_ep // 4
-    lag = 1
-    near_lag = 2
+    lag = 2
+    near_lag = 4
     part_units = units // n_tp
     k_size = width // K_CHUNKS
     d_size = width // D_CHUNKS
@@ -174,7 +175,7 @@
         return pltpu.make_async_remote_copy(
             src_ref=origin,
             dst_ref=down_b.at[(r,) + span],
-            send_sem=down_send.at[r, j],
+            send_sem=down_send.at[r],
             recv_sem=down_recv.at[r, j],
             device_id={"tp": tp ^ low},
             device_id_type=MESH,
@@ -185,9 +186,19 @@
         return pltpu.make_async_remote_copy(
             src_ref=arrived.at[u, i, r ^ low],
             dst_ref=arrived.at[u, i, r],
-            send_sem=row_send.at[r, u, i],
-            recv_sem=row_recv.at[r, u, i],
+            send_sem=row_send.at[r],
+            recv_sem=row_recv.at[relays.index(r), u, i] if r in relays else leaf_recv.at[r, u],
             device_id={"tp": tp ^ low},
+            device_id_type=MESH,
+        )
+
+    def everything(ref, send, recv):
+        return pltpu.make_async_remote_copy(
+            src_ref=ref,
+            dst_ref=ref,
+            send_sem=send,
+            recv_sem=recv,
+            device_id={"ep": peer(1)},
             device_id_type=MESH,
         )
 
@@ -264,7 +275,7 @@
         return pltpu.make_async_remote_copy(
             src_ref=outgoing.at[u, i],
             dst_ref=arrived.at[u, i, 0],
-            send_sem=out_send.at[u, i],
+            send_sem=out_send.at[half, i],
             recv_sem=out_recv.at[u, i],
             device_id={"ep": peer(half * group + i)},
             device_id_type=MESH,
@@ -289,7 +300,6 @@
             send_group(u)
     for u in range(rounds + 1, n_groups):
         send_group(u)
-    share_copy.start()
 
     for load in loads[4:]:
         load.wait()
@@ -362,18 +372,15 @@
         return pltpu.make_async_remote_copy(
             src_ref=hidden_out.at[u, r],
             dst_ref=hidden.at[u, :, :, r * part_units : (r + 1) * part_units],
-            send_sem=hid_send.at[r, u],
-            recv_sem=hid_recv.at[r, u],
+            send_sem=hid_send.at[r],
+            recv_sem=hid_recv.at[r],
             device_id={"tp": tp ^ r},
             device_id_type=MESH,
         )
 
     def work(u):
         for r in leaves:
-
-            @pl.loop(0, group)
-            def _(i):
-                row_copy(r, u, i).wait_recv()
+            everything(arrived.at[u, :, r], row_send.at[r], leaf_recv.at[r, u]).wait_recv()
 
         @pl.loop(0, K_CHUNKS)
         def _(k):
@@ -406,6 +413,8 @@
                 tail_copy(1).wait_recv()
 
             halo.start()
+        if step == len(sequence):
+            share_copy.start()
         if step == len(sequence) and step >= 2:
             work(sequence[step - 2])
             start_down(FIRST, SECOND)
@@ -418,9 +427,9 @@
     for r in range(1, n_tp):
         send_mix(r).start()
 
-    for u in sequence:
-        for r in range(1, n_tp):
-            hid_copy(r, u).wait_recv()
+    for r in range(1, n_tp):
+        mine = hidden.at[:, :, :, r * part_units : (r + 1) * part_units]
+        everything(mine, hid_send.at[r], hid_recv.at[r]).wait_recv()
 
     far = slice(rounds, n_groups)
 
@@ -428,8 +437,8 @@
         return pltpu.make_async_remote_copy(
             src_ref=result.at[j, 0:rounds, i],
             dst_ref=returned.at[j, :, i],
-            send_sem=ret_send.at[j, i],
-            recv_sem=ret_recv.at[j, i],
+            send_sem=ret_send.at[i],
+            recv_sem=ret_recv.at[j],
             device_id={"ep": peer(i)},
             device_id_type=MESH,
         )
@@ -446,8 +455,8 @@
         return pltpu.make_async_remote_copy(
             src_ref=result.at[j, far, i],
             dst_ref=gathered.at[kind, j, :, i],
-            send_sem=col_send.at[j, i],
-            recv_sem=col_recv.at[kind, j, i],
+            send_sem=col_send.at[i],
+            recv_sem=col_recv.at[kind, j],
             device_id={"ep": peer(step)},
             device_id_type=MESH,
         )
@@ -457,14 +466,11 @@
         step = lax.rem(i, quarter) + (1 - inner) * quarter
         return kind, step
 
-    def collect_in(i, kind):
-        return lax.rem(i, quarter) + (1 - jnp.bitwise_xor(bit_of(i), kind)) * quarter
-
     def partial_copy(kind, j):
         return pltpu.make_async_remote_copy(
             src_ref=partial_out.at[kind, j],
             dst_ref=partial_in.at[j],
-            send_sem=part_send.at[kind, j],
+            send_sem=part_send.at[kind],
             recv_sem=part_recv.at[j],
             device_id={"ep": peer(group + (1 - kind) * quarter)},
             device_id_type=MESH,
@@ -475,14 +481,8 @@
         def _():
             for kind in (1, 0):
 
-                @pl.loop(0, group)
-                def _(i):
-                    step = collect_in(i, kind)
-
-                    @pl.when(step > 0)
-                    def _():
-                        collect(j, i, kind, step).wait_recv()
-
+                several = gathered.at[kind, j, :, 0 : group - 1]
+                everything(several, col_send.at[0], col_recv.at[kind, j]).wait_recv()
                 rows = gathered[kind, j].reshape(slots // 2, d_size)
                 partial_out[kind, j] = (
                     jnp.dot(share_in[kind, 0], rows, preferred_element_type=jnp.float32)
@@ -585,15 +585,12 @@
 
     def write_out(j):
         return pltpu.make_async_copy(
-            e_out.at[j], expert_out.at[:, pl.ds(aligned(j, d_size), d_size)], e_store.at[j]
+            e_out.at[j], expert_out.at[:, pl.ds(aligned(j, d_size), d_size)], e_store
         )
 
     @pl.loop(0, D_CHUNKS)
     def _(j):
-        @pl.loop(1, group)
-        def _(i):
-            send_back(j, i).wait_recv()
-
+        everything(returned.at[j, :, 1:group], ret_send.at[0], ret_recv.at[j]).wait_recv()
         partial_copy(0, j).wait_recv()
         rows = returned[j].reshape(slots // 2, d_size)
         e_out[j] = (
@@ -604,61 +601,43 @@
         write_out(j).start()
 
     for r in range(1, n_tp):
-
-        @pl.loop(0, D_CHUNKS)
-        def _(j):
-            down_copy(r, j).wait_send()
-
-        @pl.loop(0, n_groups)
-        def _(u):
-            hid_copy(r, u).wait_send()
-
-        @pl.loop(0, n_groups)
-        def _(u):
-            @pl.loop(0, group)
-            def _(i):
-                row_copy(r, u, i).wait_send()
-
+        everything(down_b.at[r], down_send.at[r], down_recv.at[r, 0]).wait_send()
+        everything(hidden_out.at[:, r], hid_send.at[r], hid_recv.at[r]).wait_send()
+        everything(arrived.at[:, :, r], row_send.at[r], hid_recv.at[r]).wait_send()
         send_mix(r).wait_send()
     halo.wait_send()
+    share_copy.wait_send()
 
     @pl.when(tp == last)
     def _():
         for r in range(1, n_tp):
             tail_copy(r).wait_send()
 
-    share_copy.wait_send()
-
     for half in range(2):
+        rows_of = slice(half * rounds, (half + 1) * rounds)
 
         @pl.loop(1 - half, group)
         def _(i):
-            for u in range(half * rounds, (half + 1) * rounds):
-                send_rows(u, i).wait_send()
-
-    @pl.loop(0, D_CHUNKS)
-    def _(j):
-        @pl.loop(0, group)
-        def _(i):
-            kind, step = collect_out(j, i)
-
-            @pl.when(step > 0)
-            def _():
-                collect(j, i, kind, step).wait_send()
-
-        @pl.loop(1, group)
-        def _(i):
-            send_back(j, i).wait_send()
-
-        @pl.when(inner == 1)
+            everything(outgoing.at[rows_of, i], out_send.at[half, i], share_send).wait_send()
+
+    @pl.loop(1, group)
+    def _(i):
+        everything(result.at[:, 0:rounds, i], ret_send.at[i], share_send).wait_send()
+
+    @pl.loop(0, group)
+    def _(i):
+        _, step = collect_out(0, i)
+
+        @pl.when(step > 0)
         def _():
-            for kind in range(2):
-                partial_copy(kind, j).wait_send()
-
-    @pl.loop(0, D_CHUNKS)
-    def _(j):
-        write_out(j).wait()
-
+            everything(result.at[:, far, i], col_send.at[i], share_send).wait_send()
+
+    @pl.when(inner == 1)
+    def _():
+        for kind in range(2):
+            everything(partial_out.at[kind], part_send.at[kind], share_send).wait_send()
+
+    everything(e_out, share_send, e_store).wait_recv()
     for store in stores:
         store.wait()
 
@@ -727,21 +706,22 @@
         vmem((n_tp, tokens, group_width), bf16),
         vmem((D_CHUNKS, tokens, d_size), bf16),
         dma((10,)),
+        dma((n_tp,)),
         dma((n_tp, D_CHUNKS)),
-        dma((n_tp, D_CHUNKS)),
+        dma((2, group)),
         dma((groups, group)),
-        dma((groups, group)),
-        dma((n_tp, groups, group)),
-        dma((n_tp, groups, group)),
+        dma((n_tp,)),
+        dma((max(1, n_tp // 2 - 1), groups, group)),
         dma((n_tp, groups)),
-        dma((n_tp, groups)),
-        dma((D_CHUNKS, group)),
-        dma((D_CHUNKS, group)),
+        dma((n_tp,)),
+        dma((n_tp,)),
+        dma((group,)),
+        dma((D_CHUNKS,)),
         dma(()),
         dma((2,)),
-        dma((D_CHUNKS, group)),
-        dma((2, D_CHUNKS, group)),
+        dma((group,)),
         dma((2, D_CHUNKS)),
+        dma((2,)),
         dma((D_CHUNKS,)),
         dma((n_tp,)),
         dma((n_tp,)),
@@ -750,7 +730,7 @@
         dma(()),
         dma(()),
         dma((n_tp,)),
-        dma((D_CHUNKS,)),
+        dma(()),
     ]
     flops = 6 * slots * width * units + 2 * n_tp * tokens * group_width * group_width
     return pl.pallas_call(

time: 161 us -> 153 us (0.950)
  Pallas kernels: 157 us -> 148 us
    pallas_call x1, Pallas kernels: 157 us -> 148 us  [shards(): pl.pallas_call(functools.partial(kernel, n_ep, n_tp), out_shape=(jax.Shap...]
where the time goes in v4:
time: 153 us; the launch traced here: 152 us
  Pallas kernels  148 us (97%)
  local copies, waits for them, and re-layouts  3.32 us (2%)
    pallas_call x1, Pallas kernels, shards(): pl.pallas_call(functools.partial(kernel, n_ep, n_tp), out_shape=(jax.Shap...  148 us
    unnamed x4, local copies, waits for them, and re-layouts  3.32 us

profile of v4, /device:TPU:16, one launch (start us, length us, event | category | flops | bytes accessed | tf_op | source)
XLA Modules:
  0.0 152.3 jit_solution(10348833545868488284)
XLA Ops:
  0.6 148.3 %shard_map.122 = (bf16[512,1024]{1,0:T(8,128)(2,1)}, bf16[128,4096]{1,0:T(8,128)(2,1)}) custom-call(bf16[128,4096]{1,0:T(8,128)(2,1)} %mixer_in.1, f32[1,4096]{1,0:T(1,128)} %bitcast.4, bf16[1,1024,1024]{2,1,0:T(8,128)(2,1)} %group_weight.1, f32[1,1024]{1,0:T(1,128)} %group_scale.1, bf16[128,4096]{1,0:T(8,128)(2,1)} %expert_in.1, f32[1,4096]{1,0:T(1,128)} %bitcast.5, ...), custom_call_target="tpu_custom_call" | custom-call | flops 10737418240 | bytes 67108864 | tf_op jit(solution)/shard_map/pallas_call | solution.py:736
  149.0 0.0 copy-start
  149.0 2.4 %copy.15 = bf16[512,1024]{1,0:T(8,128)(2,1)} copy(bf16[512,1024]{1,0:T(8,128)(2,1)} %get-tuple-element.4) | data formatting | bytes 2097152
  151.3 0.0 copy-done
  151.3 1.0 copy.16
Async XLA Ops:
  149.0 2.4 %copy-start = (bf16[128,4096]{1,0:T(8,128)(2,1)S(1)}, bf16[128,4096]{1,0:T(8,128)(2,1)}, u32[]{:S(2)}) copy-start(bf16[128,4096]{1,0:T(8,128)(2,1)} %get-tuple-element.5) | copy-start | bytes 3145732

commit v5 on v4

--- a/solution.py
+++ b/solution.py
@@ -8,7 +8,7 @@
 
 WMAX = 16
 NORM_ROWS = 16
-K_CHUNKS = 8
+K_CHUNKS = 1
 D_CHUNKS = 16
 FIRST = 1
 SECOND = 2

time: 153 us -> 153 us (level)
  no operation moved by 1% of the time
where the time goes in v5:
time: 153 us; the launch traced here: 151 us
  Pallas kernels  147 us (96%)
  local copies, waits for them, and re-layouts  3.32 us (2%)
    pallas_call x1, Pallas kernels, shards(): pl.pallas_call(functools.partial(kernel, n_ep, n_tp), out_shape=(jax.Shap...  147 us
    unnamed x4, local copies, waits for them, and re-layouts  3.32 us

profile of v5, /device:TPU:16, one launch (start us, length us, event | category | flops | bytes accessed | tf_op | source)
XLA Modules:
  0.0 150.8 jit_solution(14256076629066522574)
XLA Ops:
  0.6 146.9 %shard_map.122 = (bf16[512,1024]{1,0:T(8,128)(2,1)}, bf16[128,4096]{1,0:T(8,128)(2,1)}) custom-call(bf16[128,4096]{1,0:T(8,128)(2,1)} %mixer_in.1, f32[1,4096]{1,0:T(1,128)} %bitcast.4, bf16[1,1024,1024]{2,1,0:T(8,128)(2,1)} %group_weight.1, f32[1,1024]{1,0:T(1,128)} %group_scale.1, bf16[128,4096]{1,0:T(8,128)(2,1)} %expert_in.1, f32[1,4096]{1,0:T(1,128)} %bitcast.5, ...), custom_call_target="tpu_custom_call" | custom-call | flops 10737418240 | bytes 67108864 | tf_op jit(solution)/shard_map/pallas_call | solution.py:736
  147.5 0.0 copy-start
  147.5 2.4 %copy.15 = bf16[512,1024]{1,0:T(8,128)(2,1)} copy(bf16[512,1024]{1,0:T(8,128)(2,1)} %get-tuple-element.4) | data formatting | bytes 2097152
  149.9 0.0 copy-done
  149.9 1.0 copy.16
Async XLA Ops:
  147.5 2.4 %copy-start = (bf16[128,4096]{1,0:T(8,128)(2,1)S(1)}, bf16[128,4096]{1,0:T(8,128)(2,1)}, u32[]{:S(2)}) copy-start(bf16[128,4096]{1,0:T(8,128)(2,1)} %get-tuple-element.5) | copy-start | bytes 3145732
